TPU v7x, 32 devices: a whole 2x2x4 slice. The times are simulated.
32 devices in a mesh: sp: 8 (over z, x), tp: 4 (over y, core).
Axes of the slice: x: 2, y: 2, z: 4, core: 2. Of those that a mesh axis runs over, the one named last changes fastest.
Arguments:
- tokens: bfloat16 [1024, 2048], P('sp', 'tp'), may hold values from -6 to 6
- conv_value_weight: bfloat16 [2048, 1024], P('sp', 'tp'), may hold values from -0.125 to 0.125
- conv_gate_weight: bfloat16 [2048, 1024], P('sp', 'tp'), may hold values from -0.125 to 0.125
- conv_kernel: bfloat16 [31, 1024], P(None, 'tp'), may hold values from -16 to 16
- conv_norm_gain: float32 [1024], P('tp'), may hold values from 0.1 to 1.9
- query_weight: bfloat16 [2048, 2048], P('sp', 'tp'), may hold values from -0.125 to 0.125
- key_weight: bfloat16 [2048, 2048], P('sp', 'tp'), may hold values from -0.125 to 0.125
- value_weight: bfloat16 [2048, 2048], P('sp', 'tp'), may hold values from -0.125 to 0.125
- input_gate_weight: bfloat16 [2048, 8], P(None, 'tp'), may hold values from -0.125 to 0.125
- forget_gate_weight: bfloat16 [2048, 8], P(None, 'tp'), may hold values from -0.125 to 0.125
- input_offset: float32 [1024, 8], P('sp', 'tp'), may hold values from -4 to 210
- forget_offset: float32 [1024, 8], P('sp', 'tp'), may hold values from 0 to 30
- memory_norm_gain: float32 [2048], P('tp'), may hold values from 0.1 to 1.9
- conv_out_weight: bfloat16 [1024, 2048], P('tp', 'sp'), may hold values from -0.3125 to 0.3125
- memory_out_weight: bfloat16 [2048, 2048], P('tp', 'sp'), may hold values from -0.125 to 0.125
Outputs:
- mixed: bfloat16 [1024, 2048], P('sp', 'tp')
All inputs are finite; a program needn't handle non-finite values.
Results may differ from a plain program's by a relative error of at most 0.03.
Values may be sent and summed in bfloat16 or wider, within the bound.
A program may use at most 128 MiB of HBM per device.

v0:
```python
import jax
import jax.numpy as jnp
from jax import lax
from jax.experimental import pallas as pl
from jax.experimental.pallas import tpu as pltpu
from jax.sharding import PartitionSpec as P

BLOCK = 64


EPS = 1e-06
LOWEST_LEVEL = -1e30


def shifted_2(value, axis, steps):
    count = lax.axis_size(axis)
    leading, last = (max(0, -steps), min(count, count - steps))
    return lax.ppermute(value, axis, [(source, source + steps) for source in range(leading, last)])


def carried_in(shard, axis, join, neutral):
    place = lax.axis_index(axis)
    gathered = jax.tree.map(
        lambda a, kind: lax.all_gather(a.astype(kind), axis),
        shard,
        (jnp.bfloat16, jnp.bfloat16, jnp.bfloat16, jnp.bfloat16),
    )
    state = jax.tree.map(lambda a, e: jnp.zeros_like(a) + jnp.asarray(e, a.dtype), shard, neutral)

    def one(step, state):
        return join(
            state,
            jax.tree.map(
                lambda a, own: lax.dynamic_index_in_dim(a, step, 0, False).astype(own.dtype),
                gathered,
                shard,
            ),
        )

    return lax.fori_loop(0, place, one, state)


def block_step(carry, inputs):
    state, normal, level = carry
    query, key, value, gate_in, forget_log = inputs
    length = gate_in.shape[-1]
    scale = query.shape[-1] ** (-0.5)
    causal = jnp.tril(jnp.ones((length, length), dtype=bool))
    within = jnp.cumsum(forget_log, axis=-1)
    log_weight = within[:, :, None] - within[:, None, :] + gate_in[:, None, :]
    log_weight = jnp.where(causal, log_weight, -jnp.inf)
    carried = within + level[:, None]
    top = jnp.maximum(carried, jnp.max(log_weight, axis=-1))
    weight = jnp.exp(log_weight - top[:, :, None])
    carried_weight = jnp.exp(carried - top) * scale
    scores = jnp.einsum("htd,hsd->hts", query, key, preferred_element_type=jnp.float32) * (
        scale * weight
    )
    numer = jnp.einsum(
        "hts,hse->hte", scores.astype(jnp.bfloat16), value, preferred_element_type=jnp.float32
    )
    numer = numer + carried_weight[:, :, None] * jnp.einsum(
        "hed,htd->hte", state.astype(jnp.bfloat16), query, preferred_element_type=jnp.float32
    )
    denom = jnp.sum(scores, axis=-1) + carried_weight * jnp.einsum(
        "hd,htd->ht", normal.astype(jnp.bfloat16), query, preferred_element_type=jnp.float32
    )
    result = numer / jnp.maximum(jnp.abs(denom), 1.0)[:, :, None]
    last = within[:, -1]
    end_log = last[:, None] - within + gate_in
    new_level = jnp.maximum(last + level, jnp.max(end_log, axis=-1))
    keep = jnp.exp(last + level - new_level)
    fresh = jnp.exp(end_log - new_level[:, None])
    scaled_key = (fresh[:, :, None] * key).astype(jnp.bfloat16)
    new_state = keep[:, None, None] * state + jnp.einsum(
        "hse,hsd->hed", value, scaled_key, preferred_element_type=jnp.float32
    )
    new_normal = keep[:, None] * normal + jnp.sum(scaled_key.astype(jnp.float32), axis=1)
    return ((new_state, new_normal, new_level), result)


def depthwise(extended, kernel):
    taps = kernel.shape[0]
    length = extended.shape[0] - taps + 1
    total = extended[0:length] * kernel[0]
    for index in range(1, taps):
        total = total + extended[index : index + length] * kernel[index]
    return total


def merge_states(first, second):
    first_state, first_normal, first_level, first_total = first
    second_state, second_normal, second_level, second_total = second
    shifted = first_level + second_total
    level = jnp.maximum(shifted, second_level)
    older = jnp.exp(shifted - level)
    newer = jnp.exp(second_level - level)
    state = older[:, None, None] * first_state + newer[:, None, None] * second_state
    normal = older[:, None] * first_normal + newer[:, None] * second_normal
    return (state, normal, level, first_total + second_total)


def on_device_by_position(
    tokens,
    conv_value_weight,
    conv_gate_weight,
    conv_kernel,
    conv_norm_gain,
    query_weight,
    key_weight,
    value_weight,
    input_gate_weight,
    forget_gate_weight,
    input_offset,
    forget_offset,
    memory_norm_gain,
    conv_out_weight,
    memory_out_weight,
):
    length = tokens.shape[0]
    heads_here = input_gate_weight.shape[1]
    whole = lax.all_gather(tokens, "tp", axis=1, tiled=True)
    pieces = (
        lax.all_gather(conv_value_weight, "sp", axis=0, tiled=True),
        lax.all_gather(conv_gate_weight, "sp", axis=0, tiled=True),
        lax.all_gather(query_weight, "sp", axis=0, tiled=True),
        lax.all_gather(key_weight, "sp", axis=0, tiled=True),
        lax.all_gather(value_weight, "sp", axis=0, tiled=True),
    )
    folded = tuple((jnp.dot(whole, piece, preferred_element_type=jnp.float32) for piece in pieces))
    conv_value, conv_gate, query_flat, key_flat, value_flat = folded
    gate_pre = jnp.dot(whole, input_gate_weight, preferred_element_type=jnp.float32)
    forget_pre = jnp.dot(whole, forget_gate_weight, preferred_element_type=jnp.float32)
    glu = (conv_value * jax.nn.sigmoid(conv_gate)).astype(jnp.bfloat16)
    taps = conv_kernel.shape[0]
    head_dim = query_flat.shape[1] // heads_here

    def to_heads(flat):
        return flat.astype(jnp.bfloat16).reshape(length, heads_here, head_dim).transpose(1, 0, 2)

    query = to_heads(query_flat)
    key = to_heads(key_flat)
    value = to_heads(value_flat)
    gate_in = (gate_pre + input_offset).T
    forget_log = jax.nn.log_sigmoid(forget_pre + forget_offset).T
    within = jnp.cumsum(forget_log, axis=1)
    total = within[:, -1]
    end_log = total[:, None] - within + gate_in
    local_level = jnp.max(end_log, axis=1)
    fresh = jnp.exp(end_log - local_level[:, None])
    scaled_key = (fresh[:, :, None] * key).astype(jnp.bfloat16)
    local_state = jnp.einsum("hse,hsd->hed", value, scaled_key, preferred_element_type=jnp.float32)
    local_normal = jnp.sum(scaled_key.astype(jnp.float32), axis=1)
    blank_state = (
        jnp.zeros_like(local_state),
        jnp.zeros_like(local_normal),
        jnp.full_like(local_level, LOWEST_LEVEL),
        jnp.zeros_like(total),
    )
    prior = shifted_2(glu[length - (taps - 1) :], "sp", 1)
    incoming = carried_in(
        (local_state, local_normal, local_level, total), "sp", merge_states, blank_state
    )
    extended = jnp.concatenate([prior, glu], axis=0).astype(jnp.float32)
    conv = depthwise(extended, conv_kernel.astype(jnp.float32))
    blocks = length // BLOCK

    def split(array):
        return jnp.moveaxis(array.reshape((heads_here, blocks, BLOCK) + array.shape[2:]), 1, 0)

    _, hidden = lax.scan(
        block_step,
        tuple(incoming[:3]),
        (split(query), split(key), split(value), split(gate_in), split(forget_log)),
    )
    hidden = jnp.moveaxis(hidden, 0, 1).reshape(heads_here, length, head_dim)
    hidden_squares = jnp.sum(hidden * hidden, axis=(0, 2))
    channel_sum, channel_squares, memory_squares = lax.psum(
        (jnp.sum(conv, axis=1), jnp.sum(conv * conv, axis=1), hidden_squares), "tp"
    )
    channels = conv.shape[1] * lax.axis_size("tp")
    mean = (channel_sum / channels)[:, None]
    variance = (channel_squares / channels)[:, None] - mean * mean
    conv_branch = jax.nn.silu((conv - mean) * lax.rsqrt(variance + EPS) * conv_norm_gain).astype(
        jnp.bfloat16
    )
    entries = heads_here * head_dim * lax.axis_size("tp")
    memory_scale = lax.rsqrt(memory_squares / entries + EPS)
    hidden = hidden * memory_scale[None, :, None]
    hidden = hidden * memory_norm_gain.reshape(heads_here, 1, head_dim)
    memory_branch = (
        hidden.transpose(1, 0, 2).reshape(length, heads_here * head_dim).astype(jnp.bfloat16)
    )
    conv_columns, memory_columns = (
        lax.all_gather(conv_out_weight, "sp", axis=1, tiled=True),
        lax.all_gather(memory_out_weight, "sp", axis=1, tiled=True),
    )
    contract = (((0,), (1,)), ((), ()))
    summed = lax.psum_scatter(
        (
            lax.dot_general(conv_columns, conv_branch, contract, preferred_element_type=jnp.float32)
            + lax.dot_general(
                memory_columns, memory_branch, contract, preferred_element_type=jnp.float32
            )
        ).astype(jnp.bfloat16),
        "tp",
        scatter_dimension=0,
        tiled=True,
    ).astype(jnp.float32)
    return summed.T.astype(jnp.bfloat16)


def forget_parts(forget_log):
    coarse = jnp.round(forget_log * 8.0) * 0.125
    return jnp.cumsum(coarse, axis=-1), jnp.cumsum(forget_log - coarse, axis=-1)


MESH = pl.DeviceIdType.MESH
IN_VMEM = pl.BlockSpec(memory_space=pltpu.VMEM)
ROLES = 4


class Sends:
    def __init__(self, semaphores):
        self.semaphores = semaphores
        self.started = []

    def start(self, source, target, arrival, device, *conditions):
        semaphore = self.semaphores.at[len(self.started)]
        copy = pltpu.make_async_remote_copy(
            src_ref=source,
            dst_ref=target,
            send_sem=semaphore,
            recv_sem=arrival,
            device_id=device,
            device_id_type=MESH,
        )
        self.started.append((copy, conditions))
        when(conditions, copy.start)

    def finish(self):
        for copy, conditions in self.started:
            when(conditions, copy.wait_send)


def when(conditions, action):
    if not conditions:
        action()
        return
    every = conditions[0]
    for condition in conditions[1:]:
        every = jnp.logical_and(every, condition)
    pl.when(every)(action)


def arrived(block, semaphore, *conditions):
    copy = pltpu.make_async_remote_copy(
        src_ref=block,
        dst_ref=block,
        send_sem=semaphore,
        recv_sem=semaphore,
        device_id=(lax.axis_index("sp"), lax.axis_index("tp")),
        device_id_type=MESH,
    )
    when(conditions, copy.wait_recv)


def role_of(i):
    flip = lax.rem(i // ROLES, 2)
    return lax.rem(i, ROLES) + flip * (1 - 2 * lax.rem(i, 2))


def line_order(here, count):
    order = []
    for distance in range(1, count):
        order.append((here - distance, here >= distance, here + 1, here + 1 < count))
        order.append((here + distance, here + distance < count, here - 1, here > 0))
    return order


def project_kernel(
    count,
    columns,
    tokens,
    wq,
    wk,
    wv,
    wcv,
    wcg,
    gate_weights,
    own_offsets,
    flat,
    gates,
    query,
    key,
    value,
    offsets,
    whole,
    weights,
    mine,
    send_sem,
    token_sem,
    weight_sem,
    half_sem,
    group_sem,
    offset_sem,
):
    me, tp = lax.axis_index("sp"), lax.axis_index("tp")
    layers = count // 2
    z, x, y, core = me // 2, lax.rem(me, 2), tp // 2, lax.rem(tp, 2)
    length, features = tokens.shape
    depth = wq.shape[0]
    wide = weights.shape[1]
    narrow = wide // 2
    barrier = pltpu.get_barrier_semaphore()
    y_side, core_side = (1 - y) * 2 + core, y * 2 + 1 - core
    for step in range(1, count):
        pl.semaphore_signal(
            barrier, inc=1, device_id=(lax.rem(me + step, count), tp), device_id_type=MESH
        )
    for side in (y_side, core_side):
        pl.semaphore_signal(barrier, inc=1, device_id=(me, side), device_id_type=MESH)

    def block(i, j):
        return whole.at[
            pl.ds(pl.multiple_of(i * length, length), length),
            pl.ds(pl.multiple_of(j * features, features), features),
        ]

    whole[
        pl.ds(pl.multiple_of(me * length, length), length),
        pl.ds(pl.multiple_of(tp * features, features), features),
    ] = tokens[...]
    sends = Sends(send_sem)
    rows = pl.ds(pl.multiple_of(me * depth, depth), depth)
    pl.semaphore_wait(barrier, count + 1)

    def pass_on(i, j, source, sides, *conditions):
        for device in sides:
            sends.start(source, block(i, j), token_sem.at[i, j], device, *conditions)

    x_side = z * 2 + 1 - x
    sends.start(tokens, block(me, tp), token_sem.at[me, tp], (me - 2, tp), z > 0)
    sends.start(tokens, block(me, tp), token_sem.at[me, tp], (me + 2, tp), z + 1 < layers)
    pass_on(me, tp, tokens, ((x_side, tp), (me, y_side), (me, core_side)))
    for step in range(1, count):
        device = (lax.rem(me + step, count), tp)
        sends.start(own_offsets, offsets.at[me], offset_sem.at[me], device)
    offsets[me] = own_offsets[...]

    def send_weights():
        for step in range(1, count):
            target = lax.rem(me + step, count)
            head, role = target // ROLES, role_of(target)
            device = (target, tp)
            window = pl.ds(pl.multiple_of(head * wide, wide), wide)
            for index, source in enumerate((wq, wk, wv)):
                sends.start(
                    source.at[:, window],
                    weights.at[rows, :],
                    weight_sem.at[me],
                    device,
                    role == index,
                )
            window = pl.ds(pl.multiple_of(head * narrow, narrow), narrow)
            for side, (source, semaphore) in enumerate(((wcv, weight_sem), (wcg, half_sem))):
                place = weights.at[rows, side * narrow : (side + 1) * narrow]
                sends.start(source.at[:, window], place, semaphore.at[me], device, role == 3)

    for target in range(count):
        head, role = target // ROLES, (target % ROLES) ^ (target // ROLES % 2)

        @pl.when(me == target)
        def _():
            if role < 3:
                weights[rows, :] = (wq, wk, wv)[role][:, head * wide : (head + 1) * wide]
            else:
                weights[rows, :narrow] = wcv[:, head * narrow : (head + 1) * narrow]
                weights[rows, narrow:] = wcg[:, head * narrow : (head + 1) * narrow]

    order = line_order(z, layers)
    for index, (source, there, onward, further) in enumerate(order):
        if index == layers:
            send_weights()
        i = source * 2 + x
        arrived(block(i, tp), token_sem.at[i, tp], there)
        sends.start(
            block(i, tp), block(i, tp), token_sem.at[i, tp], (onward * 2 + x, tp), there, further
        )
        pass_on(i, tp, block(i, tp), ((x_side, tp), (me, y_side), (me, core_side)), there)
    for source, there in [(z, None)] + [entry[:2] for entry in order]:
        conditions = () if there is None else (there,)
        i = source * 2 + 1 - x
        arrived(block(i, tp), token_sem.at[i, tp], *conditions)
        pass_on(i, tp, block(i, tp), ((me, y_side), (me, core_side)), *conditions)
    for step in range(count):
        i = lax.rem(me + step, count)
        arrived(block(i, y_side), token_sem.at[i, y_side])
        pass_on(i, y_side, block(i, y_side), ((me, core_side),))
    for step in range(count):
        i = lax.rem(me + step, count)
        for j in (core_side, (1 - y) * 2 + 1 - core):
            arrived(block(i, j), token_sem.at[i, j])
    role_here = role_of(me)
    for step in range(1, count):
        i = lax.rem(me + step, count)
        arrived(offsets.at[i], offset_sem.at[i])
        part = pl.ds(pl.multiple_of(i * depth, depth), depth)
        arrived(weights.at[part, :], weight_sem.at[i], role_here < 3)
        arrived(weights.at[part, :narrow], weight_sem.at[i], role_here == 3)
        arrived(weights.at[part, narrow:], half_sem.at[i], role_here == 3)

    total = flat.shape[0]
    chunk = total // ROLES
    for index in range(ROLES):
        part = slice(index * chunk, (index + 1) * chunk)
        lines = whole[part, :]
        product = jnp.dot(lines, weights[...], preferred_element_type=jnp.float32)
        flat[part, :] = product
        mine[part, :] = product.astype(jnp.bfloat16)
        gates[part, :] = jnp.dot(lines, gate_weights[...], preferred_element_type=jnp.float32)

    first = me - lax.rem(me, ROLES)
    flip = lax.rem(me // ROLES, 2)
    for role in range(ROLES):
        part = slice(role * chunk, (role + 1) * chunk)
        until = slice(0, (role + 1) * chunk)
        device = (first + role + flip * (1 - 2 * (role % 2)), tp)
        for sender, target, source in (
            (2, value.at[until, :], mine.at[until, :]),
            (1, key.at[until, :], mine.at[until, :]),
            (0, query, mine.at[part, :]),
        ):
            if sender != role:
                sends.start(source, target, group_sem.at[sender], device, role_here == sender)
            else:

                @pl.when(role_here == role)
                def _():
                    target[...] = source[...]

        @pl.when(role_here == role)
        def _():
            if (role + 1) * chunk < total:
                rest = slice((role + 1) * chunk, total)
                key[rest, :] = jnp.zeros_like(key[rest, :])
                value[rest, :] = jnp.zeros_like(value[rest, :])

    for role in range(ROLES):
        until = slice(0, (role + 1) * chunk)
        for sender, target in ((0, query), (1, key.at[until, :]), (2, value.at[until, :])):
            if sender != role:
                arrived(target, group_sem.at[sender], role_here == role)
    sends.finish()


def project(tokens, wq, wk, wv, wcv, wcg, gate_weights, own_offsets, head_dim):
    count, columns = lax.axis_size("sp"), lax.axis_size("tp")
    length, features = tokens.shape
    total = length * count
    f32, bf16 = jnp.float32, jnp.bfloat16
    shape = jax.ShapeDtypeStruct
    return pl.pallas_call(
        lambda *refs: project_kernel(count, columns, *refs),
        out_shape=(
            shape((total, head_dim), f32),
            shape((total, gate_weights.shape[1]), f32),
            shape((total // ROLES, head_dim), bf16),
            shape((total, head_dim), bf16),
            shape((total, head_dim), bf16),
            shape((count,) + own_offsets.shape, f32),
        ),
        in_specs=[IN_VMEM] * 8,
        out_specs=(IN_VMEM,) * 6,
        scratch_shapes=[
            pltpu.VMEM((total, features * columns), bf16),
            pltpu.VMEM((wq.shape[0] * count, head_dim), bf16),
            pltpu.VMEM((total, head_dim), bf16),
            pltpu.SemaphoreType.DMA((192,)),
            pltpu.SemaphoreType.DMA((count, columns)),
            pltpu.SemaphoreType.DMA((count,)),
            pltpu.SemaphoreType.DMA((count,)),
            pltpu.SemaphoreType.DMA((3,)),
            pltpu.SemaphoreType.DMA((count,)),
        ],
        compiler_params=pltpu.CompilerParams(collective_id=0, has_side_effects=True),
    )(tokens, wq, wk, wv, wcv, wcg, gate_weights, own_offsets)


def sums_kernel(count, columns, sums, total, slots, send_sem, arrival_sem):
    me, tp = lax.axis_index("sp"), lax.axis_index("tp")
    groups = count // ROLES
    members = groups * columns
    role = role_of(me)
    own = (me // ROLES) * columns + tp
    barrier = pltpu.get_barrier_semaphore()
    peers = [lax.rem(own + step, members) for step in range(1, members)]
    devices = []
    for peer in peers:
        group = peer // columns
        seat = role + lax.rem(group, 2) * (1 - 2 * lax.rem(role, 2))
        devices.append((group * ROLES + seat, lax.rem(peer, columns)))
    for device in devices:
        pl.semaphore_signal(barrier, inc=1, device_id=device, device_id_type=MESH)
    pl.semaphore_wait(barrier, members - 1)
    sends = Sends(send_sem)
    for device in devices:
        sends.start(sums, slots.at[own], arrival_sem.at[own], device)
    slots[own] = sums[...]
    for peer in peers:
        arrived(slots.at[peer], arrival_sem.at[peer])
    result = slots[0]
    for index in range(1, members):
        result = result + slots[index]
    total[...] = result
    sends.finish()


def sum_over_group(sums):
    count, columns = lax.axis_size("sp"), lax.axis_size("tp")
    members = count // ROLES * columns
    return pl.pallas_call(
        lambda *refs: sums_kernel(count, columns, *refs),
        out_shape=jax.ShapeDtypeStruct(sums.shape, sums.dtype),
        in_specs=[IN_VMEM],
        out_specs=IN_VMEM,
        scratch_shapes=[
            pltpu.VMEM((members,) + sums.shape, sums.dtype),
            pltpu.SemaphoreType.DMA((members,)),
            pltpu.SemaphoreType.DMA((members,)),
        ],
        compiler_params=pltpu.CompilerParams(collective_id=1, has_side_effects=True),
    )(sums)


def mix_kernel(
    count,
    columns,
    memory,
    conv,
    memory_weight,
    conv_weight,
    mixed,
    memories,
    convs,
    partial,
    slots,
    send_sem,
    memory_sem,
    conv_sem,
    slot_sem,
):
    me, tp = lax.axis_index("sp"), lax.axis_index("tp")
    layers = count // 2
    z, x = me // 2, lax.rem(me, 2)
    chunk = memory.shape[0]
    share = count // columns
    barrier = pltpu.get_barrier_semaphore()
    for step in range(1, count):
        pl.semaphore_signal(
            barrier, inc=1, device_id=(lax.rem(me + step, count), tp), device_id_type=MESH
        )
    inside = me // share == tp
    for half in range(share):
        for j in range(columns):
            source = tp * share + half

            @pl.when(tp != j)
            def _():
                pl.semaphore_signal(barrier, inc=1, device_id=(source, j), device_id_type=MESH)

    @pl.when(inside)
    def _():
        pl.semaphore_wait(barrier, count - 1)

    @pl.when(jnp.logical_not(inside))
    def _():
        pl.semaphore_wait(barrier, 2 * count - 1)

    def memory_at(i):
        rows = pl.multiple_of(role_of(i) * chunk, chunk)
        return memories.at[i // ROLES, pl.ds(rows, chunk), :]

    def has_conv(i):
        return role_of(i) == ROLES - 1

    sends = Sends(send_sem)

    def piece(index):
        return slice(index * chunk, (index + 1) * chunk)

    def spread_memory(i, own, device, *conditions):
        sends.start(
            memory if own else memory_at(i), memory_at(i), memory_sem.at[i], device, *conditions
        )

    def spread_conv(i, index, own, device, *conditions):
        place = convs.at[i // ROLES, piece(index), :]
        sends.start(
            conv.at[piece(index), :] if own else place,
            place,
            conv_sem.at[i, index],
            device,
            has_conv(i),
            *conditions,
        )

    def conv_arrived(i, index, *conditions):
        place = convs.at[i // ROLES, piece(index), :]
        arrived(place, conv_sem.at[i, index], has_conv(i), *conditions)

    x_side = (z * 2 + 1 - x, tp)
    below, above = (me - 2, tp), (me + 2, tp)
    spread_memory(me, True, below, z > 0)
    spread_memory(me, True, above, z + 1 < layers)
    spread_memory(me, True, x_side)
    for index in range(ROLES):
        spread_conv(me, index, True, below, z > 0)
        spread_conv(me, index, True, above, z + 1 < layers)
        spread_conv(me, index, True, x_side)
    rows_here = pl.multiple_of(role_of(me) * chunk, chunk)
    memories[me // ROLES, pl.ds(rows_here, chunk), :] = memory[...]

    @pl.when(has_conv(me))
    def _():
        convs[me // ROLES] = conv[...]

    order = line_order(z, layers)
    for source, there, onward, further in order:
        i = source * 2 + x
        arrived(memory_at(i), memory_sem.at[i], there)
        spread_memory(i, False, (onward * 2 + x, tp), there, further)
        spread_memory(i, False, x_side, there)
    for source, there, onward, further in order:
        i = source * 2 + x
        for index in range(ROLES):
            conv_arrived(i, index, there)
            spread_conv(i, index, False, (onward * 2 + x, tp), there, further)
            spread_conv(i, index, False, x_side, there)
    for source, there in [(z, z >= 0)] + [entry[:2] for entry in order]:
        i = source * 2 + 1 - x
        arrived(memory_at(i), memory_sem.at[i], there)
        for index in range(ROLES):
            conv_arrived(i, index, there)

    groups = count // ROLES
    head_dim = memory.shape[1]
    channels = conv.shape[1]
    length = mixed.shape[0]
    for index in range(ROLES):
        part = slice(index * chunk, (index + 1) * chunk)
        total = None
        for head in range(groups):
            term = jnp.dot(
                memories[head, part, :],
                memory_weight[head * head_dim : (head + 1) * head_dim, :],
                preferred_element_type=jnp.float32,
            ) + jnp.dot(
                convs[head, part, :],
                conv_weight[head * channels : (head + 1) * channels, :],
                preferred_element_type=jnp.float32,
            )
            total = term if total is None else total + term
        partial[part, :] = total.astype(jnp.bfloat16)
    column, half = me // share, lax.rem(me, share)
    for step in range(count):
        i = lax.rem(me + step, count)
        place = pl.ds(pl.multiple_of(i * length, length), length)
        away = jnp.logical_or(i != me, tp != column)
        sends.start(
            partial.at[place, :], slots.at[half, tp], slot_sem.at[half, tp], (i, column), away
        )
        if step == 0:

            @pl.when(jnp.logical_not(away))
            def _():
                slots[half, tp] = partial[place, :]

    width = partial.shape[1]
    for half in range(share):
        total = None
        for j in range(columns):
            arrived(
                slots.at[half, j],
                slot_sem.at[half, j],
                jnp.logical_or(tp * share + half != me, tp != j),
            )
        for j in range(columns):
            term = slots[half, j].astype(jnp.float32)
            total = term if total is None else total + term
        mixed[:, half * width : (half + 1) * width] = total.astype(jnp.bfloat16)
    sends.finish()


def mix(memory, conv, memory_weight, conv_weight):
    count, columns = lax.axis_size("sp"), lax.axis_size("tp")
    chunk, head_dim = memory.shape
    total, channels = conv.shape
    groups, share = count // ROLES, count // columns
    width = memory_weight.shape[1]
    length = total // count
    bf16 = jnp.bfloat16
    return pl.pallas_call(
        lambda *refs: mix_kernel(count, columns, *refs),
        out_shape=jax.ShapeDtypeStruct((length, width * share), bf16),
        in_specs=[IN_VMEM] * 4,
        out_specs=IN_VMEM,
        scratch_shapes=[
            pltpu.VMEM((groups, total, head_dim), bf16),
            pltpu.VMEM((groups, total, channels), bf16),
            pltpu.VMEM((total, width), bf16),
            pltpu.VMEM((share, columns, length, width), bf16),
            pltpu.SemaphoreType.DMA((96,)),
            pltpu.SemaphoreType.DMA((count,)),
            pltpu.SemaphoreType.DMA((count, ROLES)),
            pltpu.SemaphoreType.DMA((share, columns)),
        ],
        compiler_params=pltpu.CompilerParams(collective_id=2, has_side_effects=True),
    )(memory, conv, memory_weight, conv_weight)


def on_device_by_column(
    tokens,
    conv_value_weight,
    conv_gate_weight,
    conv_kernel,
    conv_norm_gain,
    query_weight,
    key_weight,
    value_weight,
    input_gate_weight,
    forget_gate_weight,
    input_offset,
    forget_offset,
    memory_norm_gain,
    conv_out_weight,
    memory_out_weight,
):
    f32, bf16 = jnp.float32, jnp.bfloat16
    count = lax.axis_size("sp")
    columns = lax.axis_size("tp")
    place = lax.axis_index("sp")
    heads_here = input_gate_weight.shape[1]
    head, role = place // ROLES, role_of(place)
    head_dim = query_weight.shape[1] // heads_here
    channels = conv_value_weight.shape[1] // heads_here
    gate_weights = jnp.concatenate([input_gate_weight, forget_gate_weight], axis=1)
    own_offsets = jnp.concatenate([input_offset, forget_offset], axis=1).T
    flat, gates, query, key, value, offsets = project(
        tokens,
        query_weight,
        key_weight,
        value_weight,
        conv_value_weight,
        conv_gate_weight,
        jnp.pad(gate_weights, ((0, 0), (0, 128 - 2 * heads_here))),
        jnp.pad(own_offsets, ((0, -2 * heads_here % 8), (0, 0))),
        head_dim,
    )
    length = flat.shape[0]
    offsets = offsets[:, : 2 * heads_here].transpose(1, 0, 2).reshape(2 * heads_here, length)
    gates = gates[:, : 2 * heads_here].T + offsets
    glu = (flat[:, :channels] * jax.nn.sigmoid(flat[:, channels:])).astype(bf16)
    taps = conv_kernel.shape[0]
    kernel = lax.dynamic_slice_in_dim(conv_kernel, head * channels, channels, 1).astype(f32)
    extended = jnp.concatenate([jnp.zeros((taps - 1, channels), f32), glu.astype(f32)], axis=0)
    conv = depthwise(extended, kernel)

    rows = length // ROLES
    start = role * rows
    gate_in = lax.dynamic_index_in_dim(gates[:heads_here], head, 0, False)
    forget_log = jax.nn.log_sigmoid(
        lax.dynamic_index_in_dim(gates[heads_here:], head, 0, False)
    )
    coarse, fine = forget_parts(forget_log)
    mine_coarse = lax.dynamic_slice_in_dim(coarse, start, rows)
    mine_fine = lax.dynamic_slice_in_dim(fine, start, rows)
    log_weight = (
        (mine_coarse[:, None] - coarse[None, :])
        + (mine_fine[:, None] - fine[None, :])
        + gate_in[None, :]
    )
    causal = (start + jnp.arange(rows))[:, None] >= jnp.arange(length)[None, :]
    log_weight = jnp.where(causal, log_weight, -jnp.inf)
    weight = jnp.exp(log_weight - jnp.max(log_weight, axis=1, keepdims=True))
    scores = jnp.einsum("td,sd->ts", query, key, preferred_element_type=f32) * (
        weight * head_dim ** (-0.5)
    )
    numer = jnp.dot(scores.astype(bf16), value, preferred_element_type=f32)
    denom = jnp.sum(scores, axis=1)
    cell = numer / jnp.maximum(jnp.abs(denom), 1.0)[:, None]

    squares = jnp.pad(jnp.sum(cell * cell, axis=1), (0, length - rows))
    normed = role == ROLES - 1
    sums = jnp.stack(
        [
            jnp.where(normed, jnp.sum(conv, axis=1), 0.0),
            jnp.where(normed, jnp.sum(conv * conv, axis=1), 0.0),
            squares,
        ]
    )
    sums = sum_over_group(jnp.pad(sums, ((0, 5), (0, 0))))
    total = conv_norm_gain.shape[0] * columns
    mean = sums[0] / total
    variance = sums[1] / total - mean * mean
    gain = lax.dynamic_slice_in_dim(conv_norm_gain, head * channels, channels)
    conv_branch = jax.nn.silu(
        (conv - mean[:, None]) * lax.rsqrt(variance + EPS)[:, None] * gain
    ).astype(bf16)
    entries = heads_here * head_dim * columns
    memory_scale = lax.rsqrt(sums[2, :rows] / entries + EPS)
    memory_gain = lax.dynamic_slice_in_dim(memory_norm_gain, head * head_dim, head_dim)
    memory_branch = (cell * memory_scale[:, None] * memory_gain).astype(bf16)

    return mix(memory_branch, conv_branch, memory_out_weight, conv_out_weight)


def splits_by_column(mesh, tokens, query_weight, conv_value_weight, input_gate_weight):
    count, columns = mesh.shape["sp"], mesh.shape["tp"]
    heads = input_gate_weight.shape[1]
    heads_here = heads // columns
    head_dim = query_weight.shape[1] // heads
    return (
        count == ROLES * heads_here
        and columns == 4
        and count % columns == 0
        and tokens.size * 2 <= 8 * 2**20
        and tokens.shape[0] % (count * 16) == 0
        and conv_value_weight.shape[1] * 2 == head_dim * heads
        and head_dim % 256 == 0
        and 2 * heads_here <= 128
    )


def solution(mesh):
    in_specs = (
        P("sp", "tp"),
        P("sp", "tp"),
        P("sp", "tp"),
        P(None, "tp"),
        P("tp"),
        P("sp", "tp"),
        P("sp", "tp"),
        P("sp", "tp"),
        P(None, "tp"),
        P(None, "tp"),
        P("sp", "tp"),
        P("sp", "tp"),
        P("tp"),
        P("tp", "sp"),
        P("tp", "sp"),
    )
    out_specs = P("sp", "tp")

    def run(*arrays):
        by_column = splits_by_column(mesh, arrays[0], arrays[5], arrays[1], arrays[8])
        on_device = on_device_by_column if by_column else on_device_by_position
        return jax.shard_map(
            on_device, mesh=mesh, in_specs=in_specs, out_specs=out_specs, check_vma=False
        )(*arrays)

    return run
```

profile of v0, /device:TPU:26, one launch (start us, length us, event | category | flops | bytes accessed | tf_op | source)
XLA Modules:
  0.0 140.4 jit_solution(12678173731653911965)
XLA Ops:
  0.0 0.0 copy-start.4
  0.0 0.7 copy-done.4
  0.8 0.0 copy-start.3
  0.8 0.0 copy-start.2
  0.8 0.7 copy-done.3
  1.5 0.0 copy-done.2
  1.5 0.3 copy.23
  1.8 0.0 copy-start.5
  1.8 0.0 copy-start.6
  1.8 0.9 pad.17.refs_6_
  2.8 0.0 copy-done.5
  2.8 0.0 copy-done.6
  2.8 0.6 pad.18.refs_7_
  3.4 53.1 %shard_map.145 = (f32[1024,256]{1,0:T(8,128)}, f32[1024,128]{1,0:T(8,128)}, bf16[256,256]{1,0:T(8,128)(2,1)}, bf16[1024,256]{1,0:T(8,128)(2,1)}, bf16[1024,256]{1,0:T(8,128)(2,1)}, /*index=5*/f32[8,8,128]{2,1,0:T(8,128)}) custom-call(bf16[128,512]{1,0:T(8,128)(2,1)} %refs_0_.1, bf16[256,512]{1,0:T(8,128)(2,1)} %refs_1_.1, bf16[256,512]{1,0:T(8,128)(2,1)} %refs_2_.2, ...), custom_call_target="tpu_custom_call" | custom-call | tf_op jit(solution)/shard_map/pallas_call | solution.py:463
  56.4 1.3 fusion.23
  57.8 0.0 copy-start.1
  57.8 2.4 %fusion.30 = (f32[1024]{0:T(1024)S(1)}, f32[1024]{0:T(1024)S(1)}, f32[1024,128]{1,0:T(8,128)S(1)}) fusion(f32[1024,128]{1,0:T(8,128)S(1)} %fusion.23, f32[128]{0:T(128)S(1)} %get-tuple-element.25, f32[128]{0:T(128)S(1)} %get-tuple-element.26, f32[128]{0:T(128)S(1)} %get-tuple-element.27, f32[128]{0:T(128)S(1)} %get-tuple-element.28, ...), kind=kLoop, calls=%fused_computation.108 | loop fusion | flops 8386560 | bytes 1072640 | tf_op jit(solution)/shard_map/reduce_sum | solution.py:797
  60.3 0.0 copy-start
  60.3 0.0 copy-done.1
  60.3 0.2 copy.24
  60.6 0.7 copy-done
  61.3 0.1 bitcast_add_fusion
  61.4 0.2 fusion.31
  61.6 0.0 copy-start.9
  61.6 0.6 dynamic-slice_reduce_fusion
  62.2 0.0 copy-start.10
  62.2 0.3 reduce-window.16
  62.5 0.1 slice.227
  62.6 0.1 slice_reduce_fusion.1
  62.7 0.1 add_bitcast_fusion.1
  62.8 0.1 dynamic_slice.23
  62.9 0.3 reduce-window.24
  63.2 0.1 slice.229
  63.3 0.1 slice_reduce_fusion
  63.4 0.1 add_bitcast_fusion
  63.5 0.1 dynamic_slice.24
  63.5 0.5 fusion
  64.0 0.0 copy-done.9
  64.0 0.0 copy-done.10
  64.0 0.0 copy-start.8
  64.0 0.7 fusion.32
  64.7 0.3 copy-done.8
  65.1 0.4 multiply_reduce_fusion.1
  65.5 0.6 select_maximum_fusion.refs_0_
  66.1 8.7 %shard_map.146 = f32[8,1024]{1,0:T(8,128)} custom-call(f32[8,1024]{1,0:T(8,128)} %select_maximum_fusion.refs_0_), custom_call_target="tpu_custom_call" | custom-call | tf_op jit(solution)/shard_map/pallas_call | solution.py:522
  74.8 0.8 slice_multiply_fusion.1
  75.6 0.0 copy-start.11
  75.7 0.7 copy-done.11
  76.3 0.1 dynamic_slice.28
  76.4 1.0 multiply_convert_fusion.refs_1_
  77.5 0.7 add_rsqrt_fusion.1
  78.2 0.0 copy-start.7
  78.2 0.7 copy-done.7
  78.8 0.1 dynamic_slice.27
  78.9 0.8 multiply_convert_fusion.2.refs_0_
  79.7 59.1 %shard_map.147 = bf16[128,512]{1,0:T(8,128)(2,1)} custom-call(bf16[256,256]{1,0:T(8,128)(2,1)} %multiply_convert_fusion.2.refs_0_, bf16[1024,128]{1,0:T(8,128)(2,1)} %multiply_convert_fusion.refs_1_, bf16[512,256]{1,0:T(8,128)(2,1)} %refs_2_.3, bf16[256,256]{1,0:T(8,128)(2,1)} %refs_3_.3), custom_call_target="tpu_custom_call" | custom-call | tf_op jit(solution)/shard_map/pallas_call | solution.py:703
  138.8 1.6 %copy.28 = bf16[128,512]{1,0:T(8,128)(2,1)} copy(bf16[128,512]{1,0:T(8,128)(2,1)} %shard_map.147) | data formatting | bytes 262144
  (14 shorter events, 0.2 us)
Async XLA Ops:
  0.0 0.7 copy-start.4
  0.8 0.7 copy-start.3
  0.8 0.7 copy-start.2
  1.8 0.9 copy-start.5
  1.8 0.9 copy-start.6
  57.8 2.5 %copy-start.1 = (f32[8,8,128]{2,1,0:T(8,128)S(1)}, f32[8,8,128]{2,1,0:T(8,128)}, u32[]{:S(2)}) copy-start(f32[8,8,128]{2,1,0:T(8,128)} %get-tuple-element.14) | copy-start | bytes 98308
  60.3 1.0 copy-start
  61.6 2.5 %copy-start.9 = (bf16[1024,256]{1,0:T(8,128)(2,1)S(1)}, bf16[1024,256]{1,0:T(8,128)(2,1)}, u32[]{:S(2)}) copy-start(bf16[1024,256]{1,0:T(8,128)(2,1)} %get-tuple-element.12) | copy-start | bytes 1572868
  62.2 1.8 %copy-start.10 = (bf16[256,256]{1,0:T(8,128)(2,1)S(1)}, bf16[256,256]{1,0:T(8,128)(2,1)}, u32[]{:S(2)}) copy-start(bf16[256,256]{1,0:T(8,128)(2,1)} %get-tuple-element.11) | copy-start | bytes 393220
  64.0 1.0 copy-start.8
  75.6 0.7 copy-start.11
  78.2 0.7 copy-start.7
where the time goes:
time: 141 us; the launch traced here: 140 us
  Pallas kernels  121 us (86%)
  other arithmetic  9.78 us (7%)
  local copies, waits for them, and re-layouts  8.42 us (6%)
    pallas_call x1, Pallas kernels, mix(): pl.pallas_call(lambda *refs: mix_kernel(count, columns, *refs), out_shape...  59.1 us
    pallas_call x1, Pallas kernels, project(): pl.pallas_call(lambda *refs: project_kernel(count, columns, *refs), out_s...  53.1 us
    pallas_call x1, Pallas kernels, sum_over_group(): pl.pallas_call(lambda *refs: sums_kernel(count, columns, *refs), out_shap...  8.66 us
    unnamed x25, local copies, waits for them, and re-layouts  5.45 us

commit v1 on v0

v1 whole, which is shorter than its diff:
```python
import jax
import jax.numpy as jnp
from jax import lax
from jax.experimental import pallas as pl
from jax.experimental.pallas import tpu as pltpu
from jax.sharding import PartitionSpec as P

BLOCK = 64


EPS = 1e-06
LOWEST_LEVEL = -1e30


def shifted_2(value, axis, steps):
    count = lax.axis_size(axis)
    leading, last = (max(0, -steps), min(count, count - steps))
    return lax.ppermute(value, axis, [(source, source + steps) for source in range(leading, last)])


def carried_in(shard, axis, join, neutral):
    place = lax.axis_index(axis)
    gathered = jax.tree.map(
        lambda a, kind: lax.all_gather(a.astype(kind), axis),
        shard,
        (jnp.bfloat16, jnp.bfloat16, jnp.bfloat16, jnp.bfloat16),
    )
    state = jax.tree.map(lambda a, e: jnp.zeros_like(a) + jnp.asarray(e, a.dtype), shard, neutral)

    def one(step, state):
        return join(
            state,
            jax.tree.map(
                lambda a, own: lax.dynamic_index_in_dim(a, step, 0, False).astype(own.dtype),
                gathered,
                shard,
            ),
        )

    return lax.fori_loop(0, place, one, state)


def block_step(carry, inputs):
    state, normal, level = carry
    query, key, value, gate_in, forget_log = inputs
    length = gate_in.shape[-1]
    scale = query.shape[-1] ** (-0.5)
    causal = jnp.tril(jnp.ones((length, length), dtype=bool))
    within = jnp.cumsum(forget_log, axis=-1)
    log_weight = within[:, :, None] - within[:, None, :] + gate_in[:, None, :]
    log_weight = jnp.where(causal, log_weight, -jnp.inf)
    carried = within + level[:, None]
    top = jnp.maximum(carried, jnp.max(log_weight, axis=-1))
    weight = jnp.exp(log_weight - top[:, :, None])
    carried_weight = jnp.exp(carried - top) * scale
    scores = jnp.einsum("htd,hsd->hts", query, key, preferred_element_type=jnp.float32) * (
        scale * weight
    )
    numer = jnp.einsum(
        "hts,hse->hte", scores.astype(jnp.bfloat16), value, preferred_element_type=jnp.float32
    )
    numer = numer + carried_weight[:, :, None] * jnp.einsum(
        "hed,htd->hte", state.astype(jnp.bfloat16), query, preferred_element_type=jnp.float32
    )
    denom = jnp.sum(scores, axis=-1) + carried_weight * jnp.einsum(
        "hd,htd->ht", normal.astype(jnp.bfloat16), query, preferred_element_type=jnp.float32
    )
    result = numer / jnp.maximum(jnp.abs(denom), 1.0)[:, :, None]
    last = within[:, -1]
    end_log = last[:, None] - within + gate_in
    new_level = jnp.maximum(last + level, jnp.max(end_log, axis=-1))
    keep = jnp.exp(last + level - new_level)
    fresh = jnp.exp(end_log - new_level[:, None])
    scaled_key = (fresh[:, :, None] * key).astype(jnp.bfloat16)
    new_state = keep[:, None, None] * state + jnp.einsum(
        "hse,hsd->hed", value, scaled_key, preferred_element_type=jnp.float32
    )
    new_normal = keep[:, None] * normal + jnp.sum(scaled_key.astype(jnp.float32), axis=1)
    return ((new_state, new_normal, new_level), result)


def depthwise(extended, kernel):
    taps = kernel.shape[0]
    length = extended.shape[0] - taps + 1
    total = extended[0:length] * kernel[0]
    for index in range(1, taps):
        total = total + extended[index : index + length] * kernel[index]
    return total


def merge_states(first, second):
    first_state, first_normal, first_level, first_total = first
    second_state, second_normal, second_level, second_total = second
    shifted = first_level + second_total
    level = jnp.maximum(shifted, second_level)
    older = jnp.exp(shifted - level)
    newer = jnp.exp(second_level - level)
    state = older[:, None, None] * first_state + newer[:, None, None] * second_state
    normal = older[:, None] * first_normal + newer[:, None] * second_normal
    return (state, normal, level, first_total + second_total)


def on_device_by_position(
    tokens,
    conv_value_weight,
    conv_gate_weight,
    conv_kernel,
    conv_norm_gain,
    query_weight,
    key_weight,
    value_weight,
    input_gate_weight,
    forget_gate_weight,
    input_offset,
    forget_offset,
    memory_norm_gain,
    conv_out_weight,
    memory_out_weight,
):
    length = tokens.shape[0]
    heads_here = input_gate_weight.shape[1]
    whole = lax.all_gather(tokens, "tp", axis=1, tiled=True)
    pieces = (
        lax.all_gather(conv_value_weight, "sp", axis=0, tiled=True),
        lax.all_gather(conv_gate_weight, "sp", axis=0, tiled=True),
        lax.all_gather(query_weight, "sp", axis=0, tiled=True),
        lax.all_gather(key_weight, "sp", axis=0, tiled=True),
        lax.all_gather(value_weight, "sp", axis=0, tiled=True),
    )
    folded = tuple((jnp.dot(whole, piece, preferred_element_type=jnp.float32) for piece in pieces))
    conv_value, conv_gate, query_flat, key_flat, value_flat = folded
    gate_pre = jnp.dot(whole, input_gate_weight, preferred_element_type=jnp.float32)
    forget_pre = jnp.dot(whole, forget_gate_weight, preferred_element_type=jnp.float32)
    glu = (conv_value * jax.nn.sigmoid(conv_gate)).astype(jnp.bfloat16)
    taps = conv_kernel.shape[0]
    head_dim = query_flat.shape[1] // heads_here

    def to_heads(flat):
        return flat.astype(jnp.bfloat16).reshape(length, heads_here, head_dim).transpose(1, 0, 2)

    query = to_heads(query_flat)
    key = to_heads(key_flat)
    value = to_heads(value_flat)
    gate_in = (gate_pre + input_offset).T
    forget_log = jax.nn.log_sigmoid(forget_pre + forget_offset).T
    within = jnp.cumsum(forget_log, axis=1)
    total = within[:, -1]
    end_log = total[:, None] - within + gate_in
    local_level = jnp.max(end_log, axis=1)
    fresh = jnp.exp(end_log - local_level[:, None])
    scaled_key = (fresh[:, :, None] * key).astype(jnp.bfloat16)
    local_state = jnp.einsum("hse,hsd->hed", value, scaled_key, preferred_element_type=jnp.float32)
    local_normal = jnp.sum(scaled_key.astype(jnp.float32), axis=1)
    blank_state = (
        jnp.zeros_like(local_state),
        jnp.zeros_like(local_normal),
        jnp.full_like(local_level, LOWEST_LEVEL),
        jnp.zeros_like(total),
    )
    prior = shifted_2(glu[length - (taps - 1) :], "sp", 1)
    incoming = carried_in(
        (local_state, local_normal, local_level, total), "sp", merge_states, blank_state
    )
    extended = jnp.concatenate([prior, glu], axis=0).astype(jnp.float32)
    conv = depthwise(extended, conv_kernel.astype(jnp.float32))
    blocks = length // BLOCK

    def split(array):
        return jnp.moveaxis(array.reshape((heads_here, blocks, BLOCK) + array.shape[2:]), 1, 0)

    _, hidden = lax.scan(
        block_step,
        tuple(incoming[:3]),
        (split(query), split(key), split(value), split(gate_in), split(forget_log)),
    )
    hidden = jnp.moveaxis(hidden, 0, 1).reshape(heads_here, length, head_dim)
    hidden_squares = jnp.sum(hidden * hidden, axis=(0, 2))
    channel_sum, channel_squares, memory_squares = lax.psum(
        (jnp.sum(conv, axis=1), jnp.sum(conv * conv, axis=1), hidden_squares), "tp"
    )
    channels = conv.shape[1] * lax.axis_size("tp")
    mean = (channel_sum / channels)[:, None]
    variance = (channel_squares / channels)[:, None] - mean * mean
    conv_branch = jax.nn.silu((conv - mean) * lax.rsqrt(variance + EPS) * conv_norm_gain).astype(
        jnp.bfloat16
    )
    entries = heads_here * head_dim * lax.axis_size("tp")
    memory_scale = lax.rsqrt(memory_squares / entries + EPS)
    hidden = hidden * memory_scale[None, :, None]
    hidden = hidden * memory_norm_gain.reshape(heads_here, 1, head_dim)
    memory_branch = (
        hidden.transpose(1, 0, 2).reshape(length, heads_here * head_dim).astype(jnp.bfloat16)
    )
    conv_columns, memory_columns = (
        lax.all_gather(conv_out_weight, "sp", axis=1, tiled=True),
        lax.all_gather(memory_out_weight, "sp", axis=1, tiled=True),
    )
    contract = (((0,), (1,)), ((), ()))
    summed = lax.psum_scatter(
        (
            lax.dot_general(conv_columns, conv_branch, contract, preferred_element_type=jnp.float32)
            + lax.dot_general(
                memory_columns, memory_branch, contract, preferred_element_type=jnp.float32
            )
        ).astype(jnp.bfloat16),
        "tp",
        scatter_dimension=0,
        tiled=True,
    ).astype(jnp.float32)
    return summed.T.astype(jnp.bfloat16)


MESH = pl.DeviceIdType.MESH
IN_VMEM = pl.BlockSpec(memory_space=pltpu.VMEM)
SENDS = 224
ROW_TILE = 8
LANES = 128
NT = (((1,), (1,)), ((), ()))


def when(conditions, action):
    if not conditions:
        action()
        return
    every = conditions[0]
    for condition in conditions[1:]:
        every = jnp.logical_and(every, condition)
    pl.when(every)(action)


class Sends:
    def __init__(self, semaphores):
        self.semaphores = semaphores
        self.started = []

    def start(self, source, target, arrival, device, *conditions):
        copy = pltpu.make_async_remote_copy(
            src_ref=source,
            dst_ref=target,
            send_sem=self.semaphores.at[len(self.started)],
            recv_sem=arrival,
            device_id=device,
            device_id_type=MESH,
        )
        self.started.append((copy, conditions))
        when(conditions, copy.start)

    def finish(self):
        for copy, conditions in self.started:
            when(conditions, copy.wait_send)


def arrived(block, semaphore, *conditions):
    copy = pltpu.make_async_remote_copy(
        src_ref=block,
        dst_ref=block,
        send_sem=semaphore,
        recv_sem=semaphore,
        device_id=(lax.axis_index("sp"), lax.axis_index("tp")),
        device_id_type=MESH,
    )
    when(conditions, copy.wait_recv)


def line_order(here, count):
    order = []
    for distance in range(1, count):
        order.append((here - distance, here >= distance, here + 1, here + 1 < count))
        order.append((here + distance, here + distance < count, here - 1, here > 0))
    return order


def pick(index, first, second):
    return jnp.where(jnp.full(first.shape, index, jnp.int32) == 1, second, first)


def stacked(rows, length):
    place = lax.broadcasted_iota(jnp.int32, (ROW_TILE, length), 0)
    result = jnp.zeros((ROW_TILE, length), jnp.float32)
    for index, row in enumerate(rows):
        result = jnp.where(place == index, row, result)
    return result


def as_columns(rows):
    length = rows.shape[1]
    rest = jnp.zeros((LANES - ROW_TILE, length), jnp.float32)
    return jnp.concatenate([rows, rest], axis=0).T


def as_rows(columns):
    length = columns[0].shape[0]
    place = lax.broadcasted_iota(jnp.int32, (length, LANES), 1)
    result = jnp.zeros((length, LANES), jnp.float32)
    for index, column in enumerate(columns):
        result = jnp.where(place == index, column, result)
    return result.T[:ROW_TILE]


def prefix_sums(rows):
    before = lax.broadcasted_iota(jnp.int32, (LANES, LANES), 0)
    after = lax.broadcasted_iota(jnp.int32, (LANES, LANES), 1)
    upper = (before <= after).astype(jnp.float32)
    carry = jnp.zeros((ROW_TILE, 1), jnp.float32)
    parts = []
    for start in range(0, rows.shape[1], LANES):
        part = carry + jnp.dot(
            rows[:, start : start + LANES],
            upper,
            precision=lax.Precision.HIGHEST,
            preferred_element_type=jnp.float32,
        )
        carry = part[:, LANES - 1 :]
        parts.append(part)
    return jnp.concatenate(parts, axis=1)


def layer_kernel(
    count,
    columns,
    tokens,
    wq,
    wk,
    wv,
    wcv,
    wcg,
    own_taps,
    own_conv_gain,
    own_memory_gain,
    own_input_gates,
    own_forget_gates,
    own_input_offsets,
    own_forget_offsets,
    own_memory_out,
    own_conv_out,
    slots,
    lines,
    weights,
    product,
    taps,
    conv_gain,
    memory_gain,
    input_gates,
    forget_gates,
    offsets,
    gate_rows,
    level_before,
    level_here,
    keys,
    values,
    queries,
    weight_near,
    weight_far,
    memory_done,
    squares_done,
    squares_in,
    extended,
    conv,
    sums_done,
    sums_in,
    conv_done,
    memory_in,
    conv_in,
    memory_out,
    conv_out,
    partial,
    send_sem,
    token_sem,
    weight_sem,
    own_sem,
    offset_sem,
    level_sem,
    pair_sem,
    query_sem,
    halo_sem,
    sums_sem,
    squares_sem,
    memory_sem,
    conv_sem,
    memory_out_sem,
    conv_out_sem,
    slot_sem,
):
    f32, bf16 = jnp.float32, jnp.bfloat16
    me, tp = lax.axis_index("sp"), lax.axis_index("tp")
    layers = count // 2
    z, x, y, core = me // 2, lax.rem(me, 2), tp // 2, lax.rem(tp, 2)
    side, odd = z // 2, lax.rem(z, 2)
    length, features = tokens.shape
    depth, head_dim = wq.shape[0], wq.shape[1] // 2
    channels = wcv.shape[1] // 2
    rows = 4 * length
    near, far = core == side, core != side
    first, second = x == 0, x == 1
    peer = (me, y * 2 + 1 - core)
    below, above = (me - 2, tp), (me + 2, tp)
    x_side = (z * 2 + 1 - x, tp)
    y_side = (me, (1 - y) * 2 + core)
    has_below, has_above = z > 0, z + 1 < layers
    sends = Sends(send_sem)

    barrier = pltpu.get_barrier_semaphore()
    devices = count * columns
    rank = me * columns + tp
    for step in range(1, devices):
        other = lax.rem(rank + step, devices)
        pl.semaphore_signal(
            barrier,
            inc=1,
            device_id=(other // columns, lax.rem(other, columns)),
            device_id_type=MESH,
        )

    def block(i, j):
        return lines.at[
            pl.ds(pl.multiple_of(i * length, length), length),
            pl.ds(pl.multiple_of(j * features, features), features),
        ]

    place = odd * 2 + x

    @pl.when(near)
    def _():
        lines[
            pl.ds(pl.multiple_of(place * length, length), length),
            pl.ds(pl.multiple_of(tp * features, features), features),
        ] = tokens[...]

    pl.semaphore_wait(barrier, devices - 1)

    goal = y * 2 + side
    mine, mine_sem = block(place, tp), token_sem.at[place, tp]
    sends.start(tokens, mine, mine_sem, (me - 2, goal), has_below)
    sends.start(tokens, mine, mine_sem, (me + 2, goal), has_above)
    sends.start(tokens, mine, mine_sem, (z * 2 + 1 - x, goal))
    sends.start(tokens, mine, mine_sem, (me, (1 - y) * 2 + side))
    sends.start(tokens, mine, mine_sem, peer, far)

    def piece(unit, i):
        return weights.at[
            pl.ds(pl.multiple_of(i * depth, depth), depth),
            unit * head_dim : (unit + 1) * head_dim,
        ]

    def shares(k, x_goal):
        whole = slice(k * head_dim, (k + 1) * head_dim)
        part = slice(k * channels, (k + 1) * channels)
        if x_goal == 0:
            return ((wk.at[:, whole], 0, 0), (wv.at[:, whole], 1, head_dim))
        return (
            (wq.at[:, whole], 0, 0),
            (wcv.at[:, part], 1, head_dim),
            (wcg.at[:, part], 1, head_dim + channels),
        )

    own_rows = pl.ds(pl.multiple_of(me * depth, depth), depth)

    def send_weights(k, x_goal, to_peer, *conditions):
        for source, unit, start in shares(k, x_goal):
            goal = peer if to_peer else ((core * 2 + k) * 2 + x_goal, y * 2 + unit)
            target = weights.at[own_rows, start : start + source.shape[1]]
            sends.start(source, target, weight_sem.at[unit, me], goal, *conditions)

    for k in (1, 0):
        for x_goal in range(2):
            send_weights(k, x_goal, False, core * 2 + k != z)
    for k in range(2):
        for x_goal in range(2):
            home = (core * 2 + k == z, x == x_goal)
            send_weights(k, x_goal, True, *home)

            def keep():
                for source, _, start in shares(k, x_goal):
                    weights[own_rows, start : start + source.shape[1]] = source[...]

            when(home, keep)

    for index, (source, target) in enumerate(
        (
            (own_taps, taps),
            (own_conv_gain, conv_gain),
            (own_memory_gain, memory_gain),
            (own_input_gates, input_gates),
            (own_forget_gates, forget_gates),
        )
    ):
        sends.start(source, target, own_sem.at[index], peer, near)

        @pl.when(near)
        def _():
            target[...] = source[...]

    for k in range(2):
        goal = ((core * 2 + k) * 2, y * 2 + side)
        here = jnp.logical_and(near, jnp.logical_and(first, core * 2 + k == z))
        for kind, source in enumerate((own_input_offsets, own_forget_offsets)):
            target = offsets.at[place, kind]
            sends.start(source, target, offset_sem.at[place], goal, jnp.logical_not(here))

            @pl.when(here)
            def _():
                target[...] = source[...]

    k_near = jnp.where(near, odd, 1 - core)
    groups = []
    for k in (k_near, 1 - k_near):
        source = core * 2 + k
        groups.append((source, k * 2 + x, k * 2 + 1 - x))
    for source, i, _ in groups:
        away, up = source != z, source < z
        for j in (y * 2, y * 2 + 1):
            spot, sem = block(i, j), token_sem.at[i, j]
            arrived(spot, sem, jnp.logical_or(away, j != tp))
            sends.start(spot, spot, sem, above, away, up, has_above)
            sends.start(spot, spot, sem, below, away, jnp.logical_not(up), has_below)
            sends.start(spot, spot, sem, x_side, away)
            sends.start(spot, spot, sem, y_side, away)
    for k in range(2):
        for x_goal in range(2):
            send_weights(k, x_goal, False, core * 2 + k == z, x != x_goal)
    for _, _, i in groups:
        for j in (y * 2, y * 2 + 1):
            spot, sem = block(i, j), token_sem.at[i, j]
            arrived(spot, sem)
            sends.start(spot, spot, sem, y_side)

    def both_units(i, *conditions):
        part = weights.at[pl.ds(pl.multiple_of(i * depth, depth), depth), :]
        for unit in range(2):
            conditional = (core == unit,) + conditions
            arrived(piece(unit, i), weight_sem.at[unit, i], *conditional)
            sends.start(piece(unit, i), piece(unit, i), weight_sem.at[unit, i], peer, *conditional)

    def other_unit(i, *conditions):
        for unit in range(2):
            arrived(piece(unit, i), weight_sem.at[unit, i], core != unit, *conditions)

    z_mate = side * 2 + 1 - odd
    near_sources = (z * 2 + 1 - x, z_mate * 2 + x, z_mate * 2 + 1 - x)
    for i in near_sources:
        both_units(i)
    for i in range(4):
        for j in ((1 - y) * 2, (1 - y) * 2 + 1):
            arrived(block(i, j), token_sem.at[i, j])
    for i in near_sources:
        other_unit(i)
    for unit in range(2):
        arrived(piece(unit, me), weight_sem.at[unit, me], far)

    def multiply(start, size):
        part = pl.ds(pl.multiple_of(start, size), size)
        return jnp.dot(lines[:, part], weights[part, :], preferred_element_type=f32)

    half = count // 2 * depth
    product[...] = multiply(side * half, half)

    for index, target in enumerate((taps, conv_gain, memory_gain, input_gates, forget_gates)):
        arrived(target, own_sem.at[index], far)
    for i in range(4):
        here = jnp.logical_and(near, place == i)
        arrived(offsets.at[i], offset_sem.at[i], first, jnp.logical_not(here))

    @pl.when(first)
    def _():
        gate_rows[...] = jnp.zeros_like(gate_rows)
        gate_rows[0:2, :] = input_gates[...].astype(f32)
        gate_rows[2:4, :] = forget_gates[...].astype(f32)
        gates = lax.dot_general(
            lines[...], gate_rows[...].astype(bf16), NT, preferred_element_type=f32
        ).T
        shift = [jnp.concatenate([offsets[i, kind] for i in range(4)], 1) for kind in range(2)]
        gate_in = pick(odd, gates[0:1] + shift[0][0:1], gates[1:2] + shift[0][1:2])
        forget = pick(odd, gates[2:3] + shift[1][0:1], gates[3:4] + shift[1][1:2])
        forget_log = jnp.minimum(forget, 0.0) - jnp.log1p(jnp.exp(-jnp.abs(forget)))
        coarse = jnp.round(forget_log * 8.0) * 0.125
        within = prefix_sums(stacked((coarse, forget_log - coarse), rows))
        which = lax.broadcasted_iota(jnp.int32, (ROW_TILE, rows), 0)
        level_here[...] = jnp.where(which == 2, gate_in, within)

    first_core, second_core = core == 0, core == 1
    sends.start(level_here, level_before, level_sem.at[0], peer, first, first_core)
    arrived(level_before, level_sem.at[0], first, second_core)

    @pl.when(jnp.logical_and(first, first_core))
    def _():
        level_before[...] = jnp.zeros_like(level_before)
        keys[:rows, :] = jnp.zeros_like(keys[:rows, :])
        values[:rows, :] = jnp.zeros_like(values[:rows, :])

    span = rows // 2
    scale = head_dim ** (-0.5)
    reach = (rows + span, 2 * rows)
    stores = (weight_near, weight_far)

    @pl.when(first)
    def _():
        before = level_before[...]
        which = lax.broadcasted_iota(jnp.int32, (ROW_TILE, rows), 0)
        here = level_here[...] + jnp.where(which < 2, before[:, rows - 1 :], 0.0)
        from_rows = jnp.concatenate([before, here], axis=1)
        to_columns = as_columns(here)
        tile = 64
        for start in range(0, rows, tile):
            index = start // span
            width = reach[index]
            to = to_columns[start : start + tile]
            log_weight = (
                (to[:, 0:1] - from_rows[0:1, :width])
                + (to[:, 1:2] - from_rows[1:2, :width])
                + from_rows[2:3, :width]
            )
            at = lax.broadcasted_iota(jnp.int32, (tile, width), 1)
            until = lax.broadcasted_iota(jnp.int32, (tile, width), 0) + (start + rows)
            seen = jnp.logical_and(at <= until, at >= rows * (1 - core))
            log_weight = jnp.where(seen, log_weight, -jnp.inf)
            weight = jnp.exp(log_weight - jnp.max(log_weight, axis=1, keepdims=True)) * scale
            stores[index][start - index * span : start - index * span + tile, :] = weight

    own_part = x * 2 + core

    def send_out(*conditions):
        for device in (peer, x_side):
            sends.start(
                own_memory_out,
                memory_out.at[own_part],
                memory_out_sem.at[own_part],
                device,
                *conditions,
            )
            sends.start(
                own_conv_out, conv_out.at[own_part], conv_out_sem.at[own_part], device, *conditions
            )

    send_out(first)
    memory_out[own_part] = own_memory_out[...]
    conv_out[own_part] = own_conv_out[...]

    far_pairs = (
        jnp.where(side == 0, 2, 1),
        jnp.where(side == 0, 3, 0),
    )
    for pair in far_pairs:
        both_units(pair * 2 + x)
        both_units(pair * 2 + 1 - x)
    for pair in far_pairs:
        other_unit(pair * 2)
        other_unit(pair * 2 + 1)
        product[...] += multiply(pair * 2 * depth, 2 * depth)

    @pl.when(second)
    def _():
        queries[...] = product[:, :head_dim].astype(bf16)

    for index in range(2):
        part = queries.at[index * span : (index + 1) * span, :]
        sends.start(part, part, query_sem.at[index], x_side, second)
    send_out(second)

    @pl.when(first)
    def _():
        keys[rows:, :] = product[:, :head_dim].astype(bf16)
        values[rows:, :] = product[:, head_dim:].astype(bf16)

    for index, array in enumerate((keys, values)):
        target = array.at[:rows, :]
        sends.start(array.at[rows:, :], target, pair_sem.at[index], peer, first, first_core)

    halo = extended.shape[0] - rows

    @pl.when(second)
    def _():
        gated = product[:, head_dim : head_dim + channels] * jax.nn.sigmoid(
            product[:, head_dim + channels :]
        )
        extended[halo:, :] = gated.astype(bf16).astype(f32)

    sends.start(
        extended.at[rows:, :], extended.at[:halo, :], halo_sem.at[0], peer, second, first_core
    )

    @pl.when(jnp.logical_and(second, first_core))
    def _():
        extended[:halo, :] = jnp.zeros((halo, channels), f32)

    arrived(extended.at[:halo, :], halo_sem.at[0], second, second_core)
    source_index = y * layers + z

    @pl.when(second)
    def _():
        number = taps.shape[0]
        kernel = taps[...].astype(f32)
        kernel = pick(odd, kernel[:, :channels], kernel[:, channels:])
        for start in range(0, rows, length):
            base = start + halo - (number - 1)
            total = extended[base : base + length, :] * kernel[0:1]
            for index in range(1, number):
                total = total + (
                    extended[base + index : base + index + length, :] * kernel[index : index + 1]
                )
            conv[start : start + length, :] = total
        all_rows = conv[...]
        sums_done[...] = as_rows(
            (
                jnp.sum(all_rows, axis=1, keepdims=True),
                jnp.sum(all_rows * all_rows, axis=1, keepdims=True),
            )
        )
        sums_in[source_index] = sums_done[...]

    sources = [(z_other, y_other) for z_other in range(layers) for y_other in range(2)]
    for z_other, y_other in sources:
        away = jnp.logical_or(z != z_other, y != y_other)
        sends.start(
            sums_done,
            sums_in.at[source_index],
            sums_sem.at[source_index],
            (z_other * 2 + 1, y_other * 2 + core),
            second,
            away,
        )
    for z_other, y_other in sources:
        away = jnp.logical_or(z != z_other, y != y_other)
        index = y_other * layers + z_other
        arrived(sums_in.at[index], sums_sem.at[index], second, away)

    @pl.when(second)
    def _():
        total = sums_in[0]
        for index in range(1, 2 * layers):
            total = total + sums_in[index]
        total = total * (1.0 / (2 * layers * channels))
        mean = total[0:1]
        inverse = lax.rsqrt(total[1:2] - mean * mean + EPS)
        across = as_columns(stacked((mean, inverse), rows))
        gain = conv_gain[...]
        gain = pick(odd, gain[:, :channels], gain[:, channels:])
        normed = (conv[...] - across[:, 0:1]) * across[:, 1:2] * gain
        conv_done[...] = (normed * jax.nn.sigmoid(normed)).astype(bf16)

    def spread(done, inside, semaphores, home, index):
        here, away = x == home, x != home
        kept = done.at[(2 * index + home) * length : (2 * index + home + 1) * length, :]
        given = done.at[(2 * index + 1 - home) * length : (2 * index + 2 - home) * length, :]
        part = slice(index * length, (index + 1) * length)
        target, sem = inside.at[z, part, :], semaphores.at[z, index]
        sends.start(kept, target, sem, below, here, has_below)
        sends.start(kept, target, sem, above, here, has_above)
        sends.start(given, target, sem, x_side, here)

        @pl.when(here)
        def _():
            inside[z, part, :] = kept[...]

    for index in range(2):
        spread(conv_done, conv_in, conv_sem, 1, index)

    for index, array in enumerate((keys, values)):
        arrived(array.at[:rows, :], pair_sem.at[index], first, second_core)
    squares_index = source_index
    for index in range(2):
        arrived(
            queries.at[index * span : (index + 1) * span, :], query_sem.at[index], first
        )

        @pl.when(first)
        def _():
            width = reach[index]
            gain = memory_gain[...]
            gain = pick(odd, gain[:, :head_dim], gain[:, head_dim:])
            squares = []
            for inner in range(2):
                start = index * span + inner * length
                scores = lax.dot_general(
                    queries[start : start + length, :],
                    keys[:width, :],
                    NT,
                    preferred_element_type=f32,
                )
                scores = scores * stores[index][inner * length : (inner + 1) * length, :]
                numer = jnp.dot(
                    scores.astype(bf16), values[:width, :], preferred_element_type=f32
                )
                denom = jnp.sum(scores, axis=1, keepdims=True)
                cell = numer / jnp.maximum(jnp.abs(denom), 1.0)
                memory_done[start : start + length, :] = (cell * gain).astype(bf16)
                squares.append(jnp.sum(cell * cell, axis=1, keepdims=True))
            squares_done[index] = as_rows((jnp.concatenate(squares, axis=0),))
            squares_in[squares_index, index] = squares_done[index]

        spread(memory_done, memory_in, memory_sem, 0, index)
        for z_other, y_other in sources:
            for x_other in range(2):
                away = jnp.logical_or(
                    jnp.logical_or(z != z_other, y != y_other), x != x_other
                )
                sends.start(
                    squares_done.at[index],
                    squares_in.at[squares_index, index],
                    squares_sem.at[squares_index, index],
                    (z_other * 2 + x_other, y_other * 2 + core),
                    first,
                    away,
                )

    across = (1 - x) * 2 + core
    arrived(memory_out.at[across], memory_out_sem.at[across])
    sends.start(memory_out.at[across], memory_out.at[across], memory_out_sem.at[across], peer)
    arrived(conv_out.at[across], conv_out_sem.at[across])
    sends.start(conv_out.at[across], conv_out.at[across], conv_out_sem.at[across], peer)

    order = line_order(z, layers)
    kinds = ((conv_in, conv_sem, 1), (memory_in, memory_sem, 0))
    entries = layers * 2 * head_dim
    for index in range(2):
        part = slice(index * length, (index + 1) * length)
        for inside, semaphores, home in kinds:
            away = x != home
            spot, sem = inside.at[z, part, :], semaphores.at[z, index]
            arrived(spot, sem, away)
            sends.start(spot, spot, sem, below, away, has_below)
            sends.start(spot, spot, sem, above, away, has_above)
        for source, there, onward, further in order:
            for inside, semaphores, _ in kinds:
                spot, sem = inside.at[source, part, :], semaphores.at[source, index]
                arrived(spot, sem, there)
                sends.start(spot, spot, sem, (onward * 2 + x, tp), there, further)
        for z_other, y_other in sources:
            own = jnp.logical_and(first, jnp.logical_and(z == z_other, y == y_other))
            slot = y_other * layers + z_other
            arrived(
                squares_in.at[slot, index], squares_sem.at[slot, index], jnp.logical_not(own)
            )
        if index == 0:
            for group in range(2):
                part_out = group * 2 + 1 - core
                arrived(memory_out.at[part_out], memory_out_sem.at[part_out])
                arrived(conv_out.at[part_out], conv_out_sem.at[part_out])
        total = squares_in[0, index]
        for slot in range(1, 2 * layers):
            total = total + squares_in[slot, index]
        total = pick(x, total[:, :length], total[:, length:])
        row_scale = as_columns(lax.rsqrt(total * (1.0 / entries) + EPS))[:, 0:1]
        for group in range(2):
            from_memory, from_conv = None, None
            for head in range(layers):
                where = group * 2 + head // 2
                inner = head % 2
                memory_term = jnp.dot(
                    memory_in[head, part, :],
                    memory_out[where, inner * head_dim : (inner + 1) * head_dim, :],
                    preferred_element_type=f32,
                )
                conv_term = jnp.dot(
                    conv_in[head, part, :],
                    conv_out[where, inner * channels : (inner + 1) * channels, :],
                    preferred_element_type=f32,
                )
                from_memory = memory_term if head == 0 else from_memory + memory_term
                from_conv = conv_term if head == 0 else from_conv + conv_term
            width = from_memory.shape[1]
            partial[index, :, group * width : (group + 1) * width] = (
                from_conv + row_scale * from_memory
            ).astype(bf16)
        goal = ((core * 2 + index) * 2 + x, z)
        away = jnp.logical_or(core * 2 + index != z, tp != z)
        sends.start(partial.at[index], slots.at[y], slot_sem.at[y], goal, away)

        @pl.when(jnp.logical_not(away))
        def _():
            slots[y] = partial[index]

    for y_other in range(2):
        own = jnp.logical_and(tp == z, jnp.logical_and(y == y_other, core == side))
        arrived(slots.at[y_other], slot_sem.at[y_other], jnp.logical_not(own))
    sends.finish()


def layer(arrays):
    count, columns = lax.axis_size("sp"), lax.axis_size("tp")
    (
        tokens,
        conv_value_weight,
        conv_gate_weight,
        conv_kernel,
        conv_norm_gain,
        query_weight,
        key_weight,
        value_weight,
        input_gate_weight,
        forget_gate_weight,
        input_offset,
        forget_offset,
        memory_norm_gain,
        conv_out_weight,
        memory_out_weight,
    ) = arrays
    length, features = tokens.shape
    depth, head_dim = query_weight.shape[0], query_weight.shape[1] // 2
    channels = conv_value_weight.shape[1] // 2
    wide = features * columns
    rows = length * count // 2
    layers = count // 2
    taps = conv_kernel.shape[0]
    halo = -(-(taps - 1) // ROW_TILE) * ROW_TILE
    width = memory_out_weight.shape[1]
    f32, bf16 = jnp.float32, jnp.bfloat16
    DMA = pltpu.SemaphoreType.DMA
    V = pltpu.VMEM
    return pl.pallas_call(
        lambda *refs: layer_kernel(count, columns, *refs),
        out_shape=jax.ShapeDtypeStruct((2, length, features), bf16),
        in_specs=[IN_VMEM] * 15,
        out_specs=IN_VMEM,
        scratch_shapes=[
            V((rows, wide), bf16),
            V((wide, 2 * head_dim), bf16),
            V((rows, 2 * head_dim), f32),
            V(conv_kernel.shape, bf16),
            V((1, 2 * channels), f32),
            V((1, 2 * head_dim), f32),
            V((2, wide), bf16),
            V((2, wide), bf16),
            V((4, 2, 2, length), f32),
            V((LANES, wide), f32),
            V((ROW_TILE, rows), f32),
            V((ROW_TILE, rows), f32),
            V((2 * rows, head_dim), bf16),
            V((2 * rows, head_dim), bf16),
            V((rows, head_dim), bf16),
            V((rows // 2, rows + rows // 2), f32),
            V((rows // 2, 2 * rows), f32),
            V((rows, head_dim), bf16),
            V((2, ROW_TILE, rows // 2), f32),
            V((count, 2, ROW_TILE, rows // 2), f32),
            V((halo + rows, channels), f32),
            V((rows, channels), f32),
            V((ROW_TILE, rows), f32),
            V((count, ROW_TILE, rows), f32),
            V((rows, channels), bf16),
            V((layers, rows // 2, head_dim), bf16),
            V((layers, rows // 2, channels), bf16),
            V((4, 2 * head_dim, width), bf16),
            V((4, 2 * channels, width), bf16),
            V((2, length, features), bf16),
            DMA((SENDS,)),
            DMA((4, columns)),
            DMA((2, count)),
            DMA((5,)),
            DMA((4,)),
            DMA((1,)),
            DMA((2,)),
            DMA((2,)),
            DMA((1,)),
            DMA((count,)),
            DMA((count, 2)),
            DMA((layers, 2)),
            DMA((layers, 2)),
            DMA((4,)),
            DMA((4,)),
            DMA((2,)),
        ],
        compiler_params=pltpu.CompilerParams(collective_id=0, has_side_effects=True),
    )(
        tokens,
        query_weight,
        key_weight,
        value_weight,
        conv_value_weight,
        conv_gate_weight,
        conv_kernel,
        conv_norm_gain.reshape(1, -1),
        memory_norm_gain.reshape(1, -1),
        input_gate_weight.T,
        forget_gate_weight.T,
        input_offset.T,
        forget_offset.T,
        memory_out_weight,
        conv_out_weight,
    )


def on_device_by_column(*arrays):
    slots = layer(arrays)
    return jnp.sum(slots.astype(jnp.float32), axis=0).astype(jnp.bfloat16)


def splits_by_column(mesh, tokens, query_weight, conv_value_weight, conv_kernel, input_gate_weight):
    count, columns = mesh.shape["sp"], mesh.shape["tp"]
    heads = input_gate_weight.shape[1]
    head_dim = query_weight.shape[1] // heads
    length = tokens.shape[0] // count
    return (
        count == 8
        and columns == 4
        and heads == count
        and length % LANES == 0
        and tokens.size * 2 <= 4 * 2**20
        and conv_value_weight.shape[1] * 2 == head_dim * heads
        and head_dim == 256
        and conv_kernel.shape[0] - 1 <= length
    )


def solution(mesh):
    in_specs = (
        P("sp", "tp"),
        P("sp", "tp"),
        P("sp", "tp"),
        P(None, "tp"),
        P("tp"),
        P("sp", "tp"),
        P("sp", "tp"),
        P("sp", "tp"),
        P(None, "tp"),
        P(None, "tp"),
        P("sp", "tp"),
        P("sp", "tp"),
        P("tp"),
        P("tp", "sp"),
        P("tp", "sp"),
    )
    out_specs = P("sp", "tp")

    def run(*arrays):
        by_column = splits_by_column(
            mesh, arrays[0], arrays[5], arrays[1], arrays[3], arrays[8]
        )
        on_device = on_device_by_column if by_column else on_device_by_position
        return jax.shard_map(
            on_device, mesh=mesh, in_specs=in_specs, out_specs=out_specs, check_vma=False
        )(*arrays)

    return run
```

time: 141 us -> 99.4 us (0.70)
  the two profiles are of different devices: /device:TPU:26 before, /device:TPU:8 now
where the time goes in v1:
time: 99.4 us; the launch traced here: 99.2 us
  Pallas kernels  97.5 us (98%)
  other arithmetic  1.68 us (2%)
    pallas_call x1, Pallas kernels, layer(): pl.pallas_call(lambda *refs: layer_kernel(count, columns, *refs), out_sha...  97.5 us

profile of v1, /device:TPU:8, one launch (start us, length us, event | category | flops | bytes accessed | tf_op | source)
XLA Modules:
  0.0 99.2 jit_solution(15913480373485611154)
XLA Ops:
  0.0 97.5 %shard_map.145 = bf16[2,128,512]{2,1,0:T(8,128)(2,1)} custom-call(bf16[128,512]{1,0:T(8,128)(2,1)} %refs_0_.1, bf16[256,512]{1,0:T(8,128)(2,1)} %refs_1_.1, bf16[256,512]{1,0:T(8,128)(2,1)} %refs_2_.1, bf16[256,512]{1,0:T(8,128)(2,1)} %refs_3_.1, bf16[256,256]{1,0:T(8,128)(2,1)} %refs_4_.1, bf16[256,256]{1,0:T(8,128)(2,1)} %refs_5_.1, ...), custom_call_target="tpu_custom_call" | custom-call | tf_op jit(solution)/shard_map/pallas_call | solution.py:909
  97.6 1.7 %reduce_sum.12 = bf16[128,512]{1,0:T(8,128)(2,1)} reduce(bf16[2,128,512]{2,1,0:T(8,128)(2,1)} %shard_map.145, bf16[]{:T(256)} %constant.2.clone.1), dimensions={0}, to_apply=%region_0.0 | reduce | flops 65536 | bytes 393218 | tf_op jit(solution)/shard_map/reduce_sum | solution.py:984

commit v2 on v1

--- a/solution.py
+++ b/solution.py
@@ -377,8 +377,7 @@
     squares_sem,
     memory_sem,
     conv_sem,
-    memory_out_sem,
-    conv_out_sem,
+    out_sem,
     slot_sem,
 ):
     f32, bf16 = jnp.float32, jnp.bfloat16
@@ -443,37 +442,37 @@
         ]
 
     def shares(k, x_goal):
-        whole = slice(k * head_dim, (k + 1) * head_dim)
-        part = slice(k * channels, (k + 1) * channels)
+        whole = pl.ds(pl.multiple_of(k * head_dim, head_dim), head_dim)
+        part = pl.ds(pl.multiple_of(k * channels, channels), channels)
         if x_goal == 0:
-            return ((wk.at[:, whole], 0, 0), (wv.at[:, whole], 1, head_dim))
+            return (
+                (wk.at[:, whole], 0, 0, head_dim),
+                (wv.at[:, whole], 1, head_dim, head_dim),
+            )
         return (
-            (wq.at[:, whole], 0, 0),
-            (wcv.at[:, part], 1, head_dim),
-            (wcg.at[:, part], 1, head_dim + channels),
+            (wq.at[:, whole], 0, 0, head_dim),
+            (wcv.at[:, part], 1, head_dim, channels),
+            (wcg.at[:, part], 1, head_dim + channels, channels),
         )
 
     own_rows = pl.ds(pl.multiple_of(me * depth, depth), depth)
+    z_first = (1 - core) * 2
 
     def send_weights(k, x_goal, to_peer, *conditions):
-        for source, unit, start in shares(k, x_goal):
-            goal = peer if to_peer else ((core * 2 + k) * 2 + x_goal, y * 2 + unit)
-            target = weights.at[own_rows, start : start + source.shape[1]]
+        for source, unit, start, size in shares(k, x_goal):
+            goal = peer if to_peer else ((z_first + k) * 2 + x_goal, y * 2 + unit)
+            target = weights.at[own_rows, start : start + size]
             sends.start(source, target, weight_sem.at[unit, me], goal, *conditions)
 
-    for k in (1, 0):
-        for x_goal in range(2):
-            send_weights(k, x_goal, False, core * 2 + k != z)
-    for k in range(2):
-        for x_goal in range(2):
-            home = (core * 2 + k == z, x == x_goal)
-            send_weights(k, x_goal, True, *home)
-
-            def keep():
-                for source, _, start in shares(k, x_goal):
-                    weights[own_rows, start : start + source.shape[1]] = source[...]
-
-            when(home, keep)
+    for x_goal in range(2):
+        home = (far, x == x_goal)
+        send_weights(odd, x_goal, True, *home)
+
+        def keep():
+            for source, _, start, size in shares(odd, x_goal):
+                weights[own_rows, start : start + size] = source[...]
+
+        when(home, keep)
 
     for index, (source, target) in enumerate(
         (
@@ -484,22 +483,41 @@
             (own_forget_gates, forget_gates),
         )
     ):
-        sends.start(source, target, own_sem.at[index], peer, near)
-
-        @pl.when(near)
+        sends.start(source, target, own_sem.at[index], peer, far)
+
+        @pl.when(far)
         def _():
             target[...] = source[...]
 
     for k in range(2):
-        goal = ((core * 2 + k) * 2, y * 2 + side)
-        here = jnp.logical_and(near, jnp.logical_and(first, core * 2 + k == z))
+        goal = ((z_first + k) * 2, y * 2 + side)
         for kind, source in enumerate((own_input_offsets, own_forget_offsets)):
-            target = offsets.at[place, kind]
-            sends.start(source, target, offset_sem.at[place], goal, jnp.logical_not(here))
-
-            @pl.when(here)
-            def _():
-                target[...] = source[...]
+            sends.start(source, offsets.at[place, kind], offset_sem.at[place], goal)
+
+    own_part = x * 2 + core
+    half_rows = own_memory_out.shape[0] // 2
+
+    def out_piece(part, number):
+        if number == 1:
+            return conv_out.at[part], out_sem.at[part, number]
+        start = half_rows * (number // 2)
+        return memory_out.at[part, start : start + half_rows, :], out_sem.at[part, number]
+
+    def send_out(number, *conditions):
+        if number == 1:
+            source = own_conv_out
+        else:
+            start = half_rows * (number // 2)
+            source = own_memory_out.at[start : start + half_rows, :]
+        target, sem = out_piece(own_part, number)
+        for device in (x_side, peer):
+            sends.start(source, target, sem, device, *conditions)
+
+    for x_goal in range(2):
+        send_weights(1 - odd, x_goal, False, far, x == x_goal)
+    send_out(0)
+    memory_out[own_part] = own_memory_out[...]
+    conv_out[own_part] = own_conv_out[...]
 
     k_near = jnp.where(near, odd, 1 - core)
     groups = []
@@ -515,14 +533,23 @@
             sends.start(spot, spot, sem, below, away, jnp.logical_not(up), has_below)
             sends.start(spot, spot, sem, x_side, away)
             sends.start(spot, spot, sem, y_side, away)
-    for k in range(2):
-        for x_goal in range(2):
-            send_weights(k, x_goal, False, core * 2 + k == z, x != x_goal)
+    send_out(1)
+    middle = jnp.logical_or(z == 1, z == 2)
+    for x_goal in range(2):
+        send_weights(side, x_goal, False, near, middle, x == x_goal)
     for _, _, i in groups:
         for j in (y * 2, y * 2 + 1):
             spot, sem = block(i, j), token_sem.at[i, j]
             arrived(spot, sem)
             sends.start(spot, spot, sem, y_side)
+
+    for x_goal in range(2):
+        send_weights(side, x_goal, False, near, jnp.logical_not(middle), x == x_goal)
+    for x_goal in range(2):
+        send_weights(1 - side, x_goal, False, near, x == x_goal)
+    for k in (jnp.where(near, side, 1 - odd), jnp.where(near, 1 - side, odd)):
+        for x_goal in range(2):
+            send_weights(k, x_goal, False, x != x_goal)
 
     def both_units(i, *conditions):
         part = weights.at[pl.ds(pl.multiple_of(i * depth, depth), depth), :]
@@ -536,7 +563,7 @@
             arrived(piece(unit, i), weight_sem.at[unit, i], core != unit, *conditions)
 
     z_mate = side * 2 + 1 - odd
-    near_sources = (z * 2 + 1 - x, z_mate * 2 + x, z_mate * 2 + 1 - x)
+    near_sources = (z_mate * 2 + x, z * 2 + 1 - x, z_mate * 2 + 1 - x)
     for i in near_sources:
         both_units(i)
     for i in range(4):
@@ -545,7 +572,7 @@
     for i in near_sources:
         other_unit(i)
     for unit in range(2):
-        arrived(piece(unit, me), weight_sem.at[unit, me], far)
+        arrived(piece(unit, me), weight_sem.at[unit, me], near)
 
     def multiply(start, size):
         part = pl.ds(pl.multiple_of(start, size), size)
@@ -555,10 +582,9 @@
     product[...] = multiply(side * half, half)
 
     for index, target in enumerate((taps, conv_gain, memory_gain, input_gates, forget_gates)):
-        arrived(target, own_sem.at[index], far)
+        arrived(target, own_sem.at[index], near)
     for i in range(4):
-        here = jnp.logical_and(near, place == i)
-        arrived(offsets.at[i], offset_sem.at[i], first, jnp.logical_not(here))
+        arrived(offsets.at[i], offset_sem.at[i], first)
 
     @pl.when(first)
     def _():
@@ -616,24 +642,7 @@
             weight = jnp.exp(log_weight - jnp.max(log_weight, axis=1, keepdims=True)) * scale
             stores[index][start - index * span : start - index * span + tile, :] = weight
 
-    own_part = x * 2 + core
-
-    def send_out(*conditions):
-        for device in (peer, x_side):
-            sends.start(
-                own_memory_out,
-                memory_out.at[own_part],
-                memory_out_sem.at[own_part],
-                device,
-                *conditions,
-            )
-            sends.start(
-                own_conv_out, conv_out.at[own_part], conv_out_sem.at[own_part], device, *conditions
-            )
-
-    send_out(first)
-    memory_out[own_part] = own_memory_out[...]
-    conv_out[own_part] = own_conv_out[...]
+    send_out(2, first)
 
     far_pairs = (
         jnp.where(side == 0, 2, 1),
@@ -654,7 +663,7 @@
     for index in range(2):
         part = queries.at[index * span : (index + 1) * span, :]
         sends.start(part, part, query_sem.at[index], x_side, second)
-    send_out(second)
+    send_out(2, second)
 
     @pl.when(first)
     def _():
@@ -802,28 +811,33 @@
                     away,
                 )
 
+    order = line_order(z, layers)
+
+    kinds = [(conv_in, conv_sem, 1, index) for index in range(2)]
+    kinds += [(memory_in, memory_sem, 0, index) for index in range(2)]
+    for inside, semaphores, home, index in kinds:
+        part = slice(index * length, (index + 1) * length)
+        away = x != home
+        spot, sem = inside.at[z, part, :], semaphores.at[z, index]
+        arrived(spot, sem, away)
+        sends.start(spot, spot, sem, below, away, has_below)
+        sends.start(spot, spot, sem, above, away, has_above)
     across = (1 - x) * 2 + core
-    arrived(memory_out.at[across], memory_out_sem.at[across])
-    sends.start(memory_out.at[across], memory_out.at[across], memory_out_sem.at[across], peer)
-    arrived(conv_out.at[across], conv_out_sem.at[across])
-    sends.start(conv_out.at[across], conv_out.at[across], conv_out_sem.at[across], peer)
-
-    order = line_order(z, layers)
-    kinds = ((conv_in, conv_sem, 1), (memory_in, memory_sem, 0))
+    for distance in range(1, layers):
+        for inside, semaphores, _, index in kinds:
+            part = slice(index * length, (index + 1) * length)
+            for source, there, onward, further in order[2 * distance - 2 : 2 * distance]:
+                spot, sem = inside.at[source, part, :], semaphores.at[source, index]
+                arrived(spot, sem, there)
+                sends.start(spot, spot, sem, (onward * 2 + x, tp), there, further)
+        if distance == 1:
+            for number in range(3):
+                spot, sem = out_piece(across, number)
+                arrived(spot, sem)
+                sends.start(spot, spot, sem, peer)
     entries = layers * 2 * head_dim
     for index in range(2):
         part = slice(index * length, (index + 1) * length)
-        for inside, semaphores, home in kinds:
-            away = x != home
-            spot, sem = inside.at[z, part, :], semaphores.at[z, index]
-            arrived(spot, sem, away)
-            sends.start(spot, spot, sem, below, away, has_below)
-            sends.start(spot, spot, sem, above, away, has_above)
-        for source, there, onward, further in order:
-            for inside, semaphores, _ in kinds:
-                spot, sem = inside.at[source, part, :], semaphores.at[source, index]
-                arrived(spot, sem, there)
-                sends.start(spot, spot, sem, (onward * 2 + x, tp), there, further)
         for z_other, y_other in sources:
             own = jnp.logical_and(first, jnp.logical_and(z == z_other, y == y_other))
             slot = y_other * layers + z_other
@@ -833,8 +847,8 @@
         if index == 0:
             for group in range(2):
                 part_out = group * 2 + 1 - core
-                arrived(memory_out.at[part_out], memory_out_sem.at[part_out])
-                arrived(conv_out.at[part_out], conv_out_sem.at[part_out])
+                for number in range(3):
+                    arrived(*out_piece(part_out, number))
         total = squares_in[0, index]
         for slot in range(1, 2 * layers):
             total = total + squares_in[slot, index]
@@ -843,7 +857,7 @@
         for group in range(2):
             from_memory, from_conv = None, None
             for head in range(layers):
-                where = group * 2 + head // 2
+                where = group * 2 + 1 - head // 2
                 inner = head % 2
                 memory_term = jnp.dot(
                     memory_in[head, part, :],
@@ -955,8 +969,7 @@
             DMA((count, 2)),
             DMA((layers, 2)),
             DMA((layers, 2)),
-            DMA((4,)),
-            DMA((4,)),
+            DMA((4, 3)),
             DMA((2,)),
         ],
         compiler_params=pltpu.CompilerParams(collective_id=0, has_side_effects=True),

time: 99.4 us -> 80.3 us (0.81)
  the two profiles are of different devices: /device:TPU:8 before, /device:TPU:13 now
where the time goes in v2:
time: 80.3 us; the launch traced here: 80.1 us
  Pallas kernels  78.5 us (98%)
  other arithmetic  1.68 us (2%)
    pallas_call x1, Pallas kernels, layer(): pl.pallas_call(lambda *refs: layer_kernel(count, columns, *refs), out_sha...  78.5 us
    reduce_sum x1, other arithmetic, on_device_by_column(): return jnp.sum(slots.astype(jnp.float32), axis=0).astype(jnp.bfloat16)  1.68 us

profile of v2, /device:TPU:13, one launch (start us, length us, event | category | flops | bytes accessed | tf_op | source)
XLA Modules:
  0.0 80.1 jit_solution(8773061779022175597)
XLA Ops:
  0.0 78.5 %shard_map.145 = bf16[2,128,512]{2,1,0:T(8,128)(2,1)} custom-call(bf16[128,512]{1,0:T(8,128)(2,1)} %refs_0_.1, bf16[256,512]{1,0:T(8,128)(2,1)} %refs_1_.1, bf16[256,512]{1,0:T(8,128)(2,1)} %refs_2_.1, bf16[256,512]{1,0:T(8,128)(2,1)} %refs_3_.1, bf16[256,256]{1,0:T(8,128)(2,1)} %refs_4_.1, bf16[256,256]{1,0:T(8,128)(2,1)} %refs_5_.1, ...), custom_call_target="tpu_custom_call" | custom-call | tf_op jit(solution)/shard_map/pallas_call | solution.py:923
  78.5 1.7 %reduce_sum.12 = bf16[128,512]{1,0:T(8,128)(2,1)} reduce(bf16[2,128,512]{2,1,0:T(8,128)(2,1)} %shard_map.145, bf16[]{:T(256)} %constant.2.clone.1), dimensions={0}, to_apply=%region_0.0 | reduce | flops 65536 | bytes 393218 | tf_op jit(solution)/shard_map/reduce_sum | solution.py:997

commit v3 on v2

--- a/solution.py
+++ b/solution.py
@@ -212,7 +212,7 @@
 
 MESH = pl.DeviceIdType.MESH
 IN_VMEM = pl.BlockSpec(memory_space=pltpu.VMEM)
-SENDS = 224
+SENDS = 30
 ROW_TILE = 8
 LANES = 128
 NT = (((1,), (1,)), ((), ()))
@@ -231,27 +231,36 @@
 class Sends:
     def __init__(self, semaphores):
         self.semaphores = semaphores
-        self.started = []
-
-    def start(self, source, target, arrival, device, *conditions):
+        self.waits = []
+        self.used = 0
+
+    def shared(self, *waits):
+        semaphore = self.semaphores.at[self.used]
+        self.used += 1
+        for whole, *conditions in waits:
+            self.waits.append((whole, semaphore, conditions))
+        return semaphore
+
+    def start(self, source, target, arrival, device, *conditions, leaving=None):
+        if leaving is None:
+            leaving = self.shared((source, *conditions))
         copy = pltpu.make_async_remote_copy(
             src_ref=source,
             dst_ref=target,
-            send_sem=self.semaphores.at[len(self.started)],
+            send_sem=leaving,
             recv_sem=arrival,
             device_id=device,
             device_id_type=MESH,
         )
-        self.started.append((copy, conditions))
         when(conditions, copy.start)
 
     def finish(self):
-        for copy, conditions in self.started:
-            when(conditions, copy.wait_send)
-
-
-def arrived(block, semaphore, *conditions):
-    copy = pltpu.make_async_remote_copy(
+        for whole, semaphore, conditions in self.waits:
+            when(conditions, waiting(whole, semaphore).wait_send)
+
+
+def waiting(block, semaphore):
+    return pltpu.make_async_remote_copy(
         src_ref=block,
         dst_ref=block,
         send_sem=semaphore,
@@ -259,6 +268,10 @@
         device_id=(lax.axis_index("sp"), lax.axis_index("tp")),
         device_id_type=MESH,
     )
+
+
+def arrived(block, semaphore, *conditions):
+    copy = waiting(block, semaphore)
     when(conditions, copy.wait_recv)
 
 
@@ -318,12 +331,12 @@
 def layer_kernel(
     count,
     columns,
-    tokens,
-    wq,
-    wk,
-    wv,
-    wcv,
-    wcg,
+    all_tokens,
+    all_wq,
+    all_wk,
+    all_wv,
+    all_wcv,
+    all_wcg,
     own_taps,
     own_conv_gain,
     own_memory_gain,
@@ -334,14 +347,20 @@
     own_memory_out,
     own_conv_out,
     slots,
+    tokens,
+    wq,
+    wk,
+    wv,
+    wcv,
+    wcg,
+    shifts,
     lines,
     weights,
     product,
     taps,
     conv_gain,
     memory_gain,
-    input_gates,
-    forget_gates,
+    gate_weights,
     offsets,
     gate_rows,
     level_before,
@@ -364,8 +383,10 @@
     memory_out,
     conv_out,
     partial,
+    load_sem,
     send_sem,
     token_sem,
+    y_sem,
     weight_sem,
     own_sem,
     offset_sem,
@@ -389,8 +410,11 @@
     depth, head_dim = wq.shape[0], wq.shape[1] // 2
     channels = wcv.shape[1] // 2
     rows = 4 * length
+    span = rows // 2
     near, far = core == side, core != side
     first, second = x == 0, x == 1
+    middle = jnp.logical_or(z == 1, z == 2)
+    ends = jnp.logical_not(middle)
     peer = (me, y * 2 + 1 - core)
     below, above = (me - 2, tp), (me + 2, tp)
     x_side = (z * 2 + 1 - x, tp)
@@ -416,23 +440,52 @@
             pl.ds(pl.multiple_of(j * features, features), features),
         ]
 
+    def blocks(number):
+        return lines.at[: number * length // columns, :]
+
     place = odd * 2 + x
-
-    @pl.when(near)
-    def _():
-        lines[
-            pl.ds(pl.multiple_of(place * length, length), length),
-            pl.ds(pl.multiple_of(tp * features, features), features),
-        ] = tokens[...]
-
+    own_part = x * 2 + core
+    loads = []
+    for source, target, *conditions in (
+        (all_tokens, tokens),
+        (all_tokens, block(place, tp), near),
+        (all_wq, wq),
+        (all_wk, wk),
+        (all_wv, wv),
+        (all_wcv, wcv),
+        (all_wcg, wcg),
+        (own_input_offsets, shifts.at[0]),
+        (own_forget_offsets, shifts.at[1]),
+        (own_taps, taps, far),
+        (own_conv_gain, conv_gain, far),
+        (own_memory_gain, memory_gain, far),
+        (own_input_gates, gate_weights.at[0], far),
+        (own_forget_gates, gate_weights.at[1], far),
+        (own_memory_out, memory_out.at[own_part]),
+        (own_conv_out, conv_out.at[own_part]),
+    ):
+        copy = pltpu.make_async_copy(source, target, load_sem.at[len(loads)])
+        loads.append((copy, conditions))
+        when(conditions, copy.start)
+
+    def loaded(first_load, last_load):
+        for copy, conditions in loads[first_load:last_load]:
+            when(conditions, copy.wait)
+
+    loaded(0, 2)
     pl.semaphore_wait(barrier, devices - 1)
 
     goal = y * 2 + side
-    mine, mine_sem = block(place, tp), token_sem.at[place, tp]
-    sends.start(tokens, mine, mine_sem, (me - 2, goal), has_below)
-    sends.start(tokens, mine, mine_sem, (me + 2, goal), has_above)
-    sends.start(tokens, mine, mine_sem, (z * 2 + 1 - x, goal))
-    sends.start(tokens, mine, mine_sem, (me, (1 - y) * 2 + side))
+    mine, mine_sem = block(place, tp), token_sem.at[place, core]
+    z_leaving = sends.shared(
+        (blocks(1), ends), (blocks(4), middle, near), (blocks(6), middle, far)
+    )
+    x_leaving = sends.shared((blocks(3), near), (blocks(5), far))
+    y_leaving = sends.shared((blocks(7), near), (blocks(9), far))
+    sends.start(tokens, mine, mine_sem, (me - 2, goal), has_below, leaving=z_leaving)
+    sends.start(tokens, mine, mine_sem, (me + 2, goal), has_above, leaving=z_leaving)
+    sends.start(tokens, mine, mine_sem, (z * 2 + 1 - x, goal), leaving=x_leaving)
+    sends.start(tokens, mine, y_sem.at[0], (me, (1 - y) * 2 + side), leaving=y_leaving)
     sends.start(tokens, mine, mine_sem, peer, far)
 
     def piece(unit, i):
@@ -457,67 +510,54 @@
 
     own_rows = pl.ds(pl.multiple_of(me * depth, depth), depth)
     z_first = (1 - core) * 2
-
-    def send_weights(k, x_goal, to_peer, *conditions):
-        for source, unit, start, size in shares(k, x_goal):
-            goal = peer if to_peer else ((z_first + k) * 2 + x_goal, y * 2 + unit)
-            target = weights.at[own_rows, start : start + size]
-            sends.start(source, target, weight_sem.at[unit, me], goal, *conditions)
-
+    share = weights.at[:depth, :]
+
+    def send_weights(k, cross, leaving, *conditions, to_peer=False):
+        for x_goal in range(2):
+            chosen = conditions + ((x != x_goal) if cross else (x == x_goal),)
+            for source, unit, start, size in shares(k, x_goal):
+                device = peer if to_peer else ((z_first + k) * 2 + x_goal, y * 2 + unit)
+                target = weights.at[own_rows, start : start + size]
+                sends.start(
+                    source, target, weight_sem.at[unit, me], device, *chosen, leaving=leaving
+                )
+
+    loaded(2, len(loads))
+    mate_leaving, other_leaving = sends.shared((share,)), sends.shared((share,))
+    send_weights(odd, False, other_leaving, far, to_peer=True)
+    send_weights(1 - odd, False, mate_leaving, far)
     for x_goal in range(2):
-        home = (far, x == x_goal)
-        send_weights(odd, x_goal, True, *home)
 
         def keep():
             for source, _, start, size in shares(odd, x_goal):
                 weights[own_rows, start : start + size] = source[...]
 
-        when(home, keep)
-
-    for index, (source, target) in enumerate(
-        (
-            (own_taps, taps),
-            (own_conv_gain, conv_gain),
-            (own_memory_gain, memory_gain),
-            (own_input_gates, input_gates),
-            (own_forget_gates, forget_gates),
-        )
-    ):
-        sends.start(source, target, own_sem.at[index], peer, far)
-
-        @pl.when(far)
-        def _():
-            target[...] = source[...]
-
+        when((far, x == x_goal), keep)
+
+    own_arrays = (taps, conv_gain, memory_gain, gate_weights)
+    for index, array in enumerate(own_arrays):
+        sends.start(array, array, own_sem.at[index], peer, far)
+    leaving = sends.shared((offsets.at[:2],))
     for k in range(2):
-        goal = ((z_first + k) * 2, y * 2 + side)
-        for kind, source in enumerate((own_input_offsets, own_forget_offsets)):
-            sends.start(source, offsets.at[place, kind], offset_sem.at[place], goal)
-
-    own_part = x * 2 + core
-    half_rows = own_memory_out.shape[0] // 2
+        device = ((z_first + k) * 2, y * 2 + side)
+        sends.start(shifts, offsets.at[place], offset_sem.at[0], device, leaving=leaving)
+
+    half_rows = memory_out.shape[1] // 2
+    out_width = memory_out.shape[2]
+    three_pieces = weights.at[: 3 * half_rows * out_width // (2 * head_dim), :]
 
     def out_piece(part, number):
         if number == 1:
-            return conv_out.at[part], out_sem.at[part, number]
+            return conv_out.at[part]
         start = half_rows * (number // 2)
-        return memory_out.at[part, start : start + half_rows, :], out_sem.at[part, number]
+        return memory_out.at[part, start : start + half_rows, :]
+
+    out_leaving = [sends.shared((three_pieces,)) for _ in range(2)]
 
     def send_out(number, *conditions):
-        if number == 1:
-            source = own_conv_out
-        else:
-            start = half_rows * (number // 2)
-            source = own_memory_out.at[start : start + half_rows, :]
-        target, sem = out_piece(own_part, number)
-        for device in (x_side, peer):
-            sends.start(source, target, sem, device, *conditions)
-
-    for x_goal in range(2):
-        send_weights(1 - odd, x_goal, False, far, x == x_goal)
-    send_out(0)
-    memory_out[own_part] = own_memory_out[...]
-    conv_out[own_part] = own_conv_out[...]
+        spot = out_piece(own_part, number)
+        for device, leaving in zip((x_side, peer), out_leaving):
+            sends.start(spot, spot, out_sem.at[own_part], device, *conditions, leaving=leaving)
 
     k_near = jnp.where(near, odd, 1 - core)
     groups = []
@@ -526,71 +566,39 @@
         groups.append((source, k * 2 + x, k * 2 + 1 - x))
     for source, i, _ in groups:
         away, up = source != z, source < z
-        for j in (y * 2, y * 2 + 1):
-            spot, sem = block(i, j), token_sem.at[i, j]
-            arrived(spot, sem, jnp.logical_or(away, j != tp))
-            sends.start(spot, spot, sem, above, away, up, has_above)
-            sends.start(spot, spot, sem, below, away, jnp.logical_not(up), has_below)
-            sends.start(spot, spot, sem, x_side, away)
-            sends.start(spot, spot, sem, y_side, away)
-    send_out(1)
-    middle = jnp.logical_or(z == 1, z == 2)
-    for x_goal in range(2):
-        send_weights(side, x_goal, False, near, middle, x == x_goal)
+        onward = (jnp.where(up, z + 1, z - 1) * 2 + x, tp)
+        for j in range(2):
+            spot, sem = block(i, y * 2 + j), token_sem.at[i, j]
+            arrived(spot, sem, jnp.logical_or(away, j != core))
+            sends.start(spot, spot, sem, onward, away, middle, leaving=z_leaving)
+            sends.start(spot, spot, sem, x_side, away, leaving=x_leaving)
+            sends.start(spot, spot, y_sem.at[0], y_side, away, leaving=y_leaving)
+    send_weights(side, False, mate_leaving, near, middle)
     for _, _, i in groups:
-        for j in (y * 2, y * 2 + 1):
-            spot, sem = block(i, j), token_sem.at[i, j]
+        for j in range(2):
+            spot, sem = block(i, y * 2 + j), token_sem.at[i, j]
             arrived(spot, sem)
-            sends.start(spot, spot, sem, y_side)
-
-    for x_goal in range(2):
-        send_weights(side, x_goal, False, near, jnp.logical_not(middle), x == x_goal)
-    for x_goal in range(2):
-        send_weights(1 - side, x_goal, False, near, x == x_goal)
-    for k in (jnp.where(near, side, 1 - odd), jnp.where(near, 1 - side, odd)):
-        for x_goal in range(2):
-            send_weights(k, x_goal, False, x != x_goal)
-
-    def both_units(i, *conditions):
-        part = weights.at[pl.ds(pl.multiple_of(i * depth, depth), depth), :]
-        for unit in range(2):
-            conditional = (core == unit,) + conditions
-            arrived(piece(unit, i), weight_sem.at[unit, i], *conditional)
-            sends.start(piece(unit, i), piece(unit, i), weight_sem.at[unit, i], peer, *conditional)
-
-    def other_unit(i, *conditions):
-        for unit in range(2):
-            arrived(piece(unit, i), weight_sem.at[unit, i], core != unit, *conditions)
-
-    z_mate = side * 2 + 1 - odd
-    near_sources = (z_mate * 2 + x, z * 2 + 1 - x, z_mate * 2 + 1 - x)
-    for i in near_sources:
-        both_units(i)
-    for i in range(4):
-        for j in ((1 - y) * 2, (1 - y) * 2 + 1):
-            arrived(block(i, j), token_sem.at[i, j])
-    for i in near_sources:
-        other_unit(i)
-    for unit in range(2):
-        arrived(piece(unit, me), weight_sem.at[unit, me], near)
-
-    def multiply(start, size):
-        part = pl.ds(pl.multiple_of(start, size), size)
-        return jnp.dot(lines[:, part], weights[part, :], preferred_element_type=f32)
-
-    half = count // 2 * depth
-    product[...] = multiply(side * half, half)
-
-    for index, target in enumerate((taps, conv_gain, memory_gain, input_gates, forget_gates)):
-        arrived(target, own_sem.at[index], near)
-    for i in range(4):
-        arrived(offsets.at[i], offset_sem.at[i], first)
+            sends.start(spot, spot, y_sem.at[0], y_side, leaving=y_leaving)
+
+    send_weights(side, False, mate_leaving, near, ends)
+    send_weights(1 - side, False, other_leaving, near)
+    for k in (jnp.where(near, 1 - side, 1 - odd), jnp.where(near, side, odd)):
+        send_weights(k, True, sends.shared((share,)))
+    for number in range(3):
+        send_out(number, first)
+    for number in range(2):
+        send_out(number, second, near)
+
+    arrived(blocks(8), y_sem.at[0])
+    for index, array in enumerate(own_arrays):
+        arrived(array, own_sem.at[index], near)
+    arrived(offsets, offset_sem.at[0], first)
 
     @pl.when(first)
     def _():
         gate_rows[...] = jnp.zeros_like(gate_rows)
-        gate_rows[0:2, :] = input_gates[...].astype(f32)
-        gate_rows[2:4, :] = forget_gates[...].astype(f32)
+        gate_rows[0:2, :] = gate_weights[0].astype(f32)
+        gate_rows[2:4, :] = gate_weights[1].astype(f32)
         gates = lax.dot_general(
             lines[...], gate_rows[...].astype(bf16), NT, preferred_element_type=f32
         ).T
@@ -605,7 +613,6 @@
 
     first_core, second_core = core == 0, core == 1
     sends.start(level_here, level_before, level_sem.at[0], peer, first, first_core)
-    arrived(level_before, level_sem.at[0], first, second_core)
 
     @pl.when(jnp.logical_and(first, first_core))
     def _():
@@ -613,13 +620,11 @@
         keys[:rows, :] = jnp.zeros_like(keys[:rows, :])
         values[:rows, :] = jnp.zeros_like(values[:rows, :])
 
-    span = rows // 2
     scale = head_dim ** (-0.5)
     reach = (rows + span, 2 * rows)
     stores = (weight_near, weight_far)
 
-    @pl.when(first)
-    def _():
+    def position_weights():
         before = level_before[...]
         which = lax.broadcasted_iota(jnp.int32, (ROW_TILE, rows), 0)
         here = level_here[...] + jnp.where(which < 2, before[:, rows - 1 :], 0.0)
@@ -642,16 +647,40 @@
             weight = jnp.exp(log_weight - jnp.max(log_weight, axis=1, keepdims=True)) * scale
             stores[index][start - index * span : start - index * span + tile, :] = weight
 
-    send_out(2, first)
-
-    far_pairs = (
-        jnp.where(side == 0, 2, 1),
-        jnp.where(side == 0, 3, 0),
-    )
-    for pair in far_pairs:
-        both_units(pair * 2 + x)
-        both_units(pair * 2 + 1 - x)
-    for pair in far_pairs:
+    forward_leaving = sends.shared((weights.at[: 7 * depth // 2, :],))
+
+    def own_unit(i):
+        for unit in range(2):
+            spot, sem = piece(unit, i), weight_sem.at[unit, i]
+            arrived(spot, sem, core == unit)
+            sends.start(spot, spot, sem, peer, core == unit, leaving=forward_leaving)
+
+    def other_unit(i):
+        for unit in range(2):
+            arrived(piece(unit, i), weight_sem.at[unit, i], core != unit)
+
+    def multiply(start, size):
+        part = pl.ds(pl.multiple_of(start, size), size)
+        return jnp.dot(lines[:, part], weights[part, :], preferred_element_type=f32)
+
+    z_mate = side * 2 + 1 - odd
+    z_far = (jnp.where(side == 0, 3, 0), jnp.where(side == 0, 2, 1))
+    own_unit(z_mate * 2 + x)
+    own_unit(z_far[0] * 2 + x)
+    arrived(level_before, level_sem.at[0], first, second_core)
+    when((first,), position_weights)
+    for i in (z * 2 + 1 - x, z_mate * 2 + 1 - x):
+        own_unit(i)
+    for i in (z_mate * 2 + x, z * 2 + 1 - x, z_mate * 2 + 1 - x):
+        other_unit(i)
+    for unit in range(2):
+        arrived(piece(unit, me), weight_sem.at[unit, me], near)
+    half = count // 2 * depth
+    product[...] = multiply(side * half, half)
+    own_unit(z_far[0] * 2 + 1 - x)
+    own_unit(z_far[1] * 2 + x)
+    own_unit(z_far[1] * 2 + 1 - x)
+    for pair in z_far:
         other_unit(pair * 2)
         other_unit(pair * 2 + 1)
         product[...] += multiply(pair * 2 * depth, 2 * depth)
@@ -660,19 +689,27 @@
     def _():
         queries[...] = product[:, :head_dim].astype(bf16)
 
+    leaving = sends.shared((queries, second))
     for index in range(2):
         part = queries.at[index * span : (index + 1) * span, :]
-        sends.start(part, part, query_sem.at[index], x_side, second)
-    send_out(2, second)
+        sends.start(part, part, query_sem.at[index], x_side, second, leaving=leaving)
 
     @pl.when(first)
     def _():
         keys[rows:, :] = product[:, :head_dim].astype(bf16)
         values[rows:, :] = product[:, head_dim:].astype(bf16)
 
-    for index, array in enumerate((keys, values)):
-        target = array.at[:rows, :]
-        sends.start(array.at[rows:, :], target, pair_sem.at[index], peer, first, first_core)
+    leaving = sends.shared((keys, first, first_core))
+    for array in (keys, values):
+        sends.start(
+            array.at[rows:, :],
+            array.at[:rows, :],
+            pair_sem.at[0],
+            peer,
+            first,
+            first_core,
+            leaving=leaving,
+        )
 
     halo = extended.shape[0] - rows
 
@@ -708,29 +745,33 @@
                 )
             conv[start : start + length, :] = total
         all_rows = conv[...]
-        sums_done[...] = as_rows(
+        both = as_rows(
             (
                 jnp.sum(all_rows, axis=1, keepdims=True),
                 jnp.sum(all_rows * all_rows, axis=1, keepdims=True),
             )
         )
+        sums_done[...] = jnp.concatenate(
+            [both[:2, start : start + LANES] for start in range(0, rows, LANES)], axis=0
+        )
         sums_in[source_index] = sums_done[...]
 
     sources = [(z_other, y_other) for z_other in range(layers) for y_other in range(2)]
+    others = sums_in.at[: count - 1]
+    leaving = sends.shared((others, second))
     for z_other, y_other in sources:
         away = jnp.logical_or(z != z_other, y != y_other)
+        device = (z_other * 2 + 1, y_other * 2 + core)
         sends.start(
             sums_done,
             sums_in.at[source_index],
-            sums_sem.at[source_index],
-            (z_other * 2 + 1, y_other * 2 + core),
+            sums_sem.at[0],
+            device,
             second,
             away,
+            leaving=leaving,
         )
-    for z_other, y_other in sources:
-        away = jnp.logical_or(z != z_other, y != y_other)
-        index = y_other * layers + z_other
-        arrived(sums_in.at[index], sums_sem.at[index], second, away)
+    arrived(others, sums_sem.at[0], second)
 
     @pl.when(second)
     def _():
@@ -738,6 +779,7 @@
         for index in range(1, 2 * layers):
             total = total + sums_in[index]
         total = total * (1.0 / (2 * layers * channels))
+        total = jnp.concatenate([total[at : at + 2] for at in range(0, ROW_TILE, 2)], axis=1)
         mean = total[0:1]
         inverse = lax.rsqrt(total[1:2] - mean * mean + EPS)
         across = as_columns(stacked((mean, inverse), rows))
@@ -746,15 +788,24 @@
         normed = (conv[...] - across[:, 0:1]) * across[:, 1:2] * gain
         conv_done[...] = (normed * jax.nn.sigmoid(normed)).astype(bf16)
 
+    piece_rows = span * (head_dim + channels) // (2 * head_dim)
+
+    def so_many(number):
+        return weights.at[: number * piece_rows, :]
+
+    up_leaving = sends.shared(*((so_many(at + 1), z == at) for at in range(layers - 1)))
+    down_leaving = sends.shared(*((so_many(layers - at), z == at) for at in range(1, layers)))
+    given_leaving = sends.shared((memory_in.at[0], first), (conv_in.at[0], second))
+
     def spread(done, inside, semaphores, home, index):
-        here, away = x == home, x != home
+        here = x == home
         kept = done.at[(2 * index + home) * length : (2 * index + home + 1) * length, :]
         given = done.at[(2 * index + 1 - home) * length : (2 * index + 2 - home) * length, :]
         part = slice(index * length, (index + 1) * length)
         target, sem = inside.at[z, part, :], semaphores.at[z, index]
-        sends.start(kept, target, sem, below, here, has_below)
-        sends.start(kept, target, sem, above, here, has_above)
-        sends.start(given, target, sem, x_side, here)
+        sends.start(given, target, sem, x_side, here, leaving=given_leaving)
+        sends.start(kept, target, sem, below, here, has_below, leaving=down_leaving)
+        sends.start(kept, target, sem, above, here, has_above, leaving=up_leaving)
 
         @pl.when(here)
         def _():
@@ -762,10 +813,12 @@
 
     for index in range(2):
         spread(conv_done, conv_in, conv_sem, 1, index)
-
-    for index, array in enumerate((keys, values)):
-        arrived(array.at[:rows, :], pair_sem.at[index], first, second_core)
-    squares_index = source_index
+    for number in range(2):
+        send_out(number, second, far)
+    send_out(2, second)
+
+    for array in (keys,):
+        arrived(array, pair_sem.at[0], first, second_core)
     for index in range(2):
         arrived(
             queries.at[index * span : (index + 1) * span, :], query_sem.at[index], first
@@ -776,7 +829,6 @@
             width = reach[index]
             gain = memory_gain[...]
             gain = pick(odd, gain[:, :head_dim], gain[:, head_dim:])
-            squares = []
             for inner in range(2):
                 start = index * span + inner * length
                 scores = lax.dot_general(
@@ -792,68 +844,92 @@
                 denom = jnp.sum(scores, axis=1, keepdims=True)
                 cell = numer / jnp.maximum(jnp.abs(denom), 1.0)
                 memory_done[start : start + length, :] = (cell * gain).astype(bf16)
-                squares.append(jnp.sum(cell * cell, axis=1, keepdims=True))
-            squares_done[index] = as_rows((jnp.concatenate(squares, axis=0),))
-            squares_in[squares_index, index] = squares_done[index]
+                square = as_rows((jnp.sum(cell * cell, axis=1, keepdims=True),))
+                squares_done[index, inner] = square[0:1]
+            squares_in[index * count + source_index] = squares_done[index, 0]
 
         spread(memory_done, memory_in, memory_sem, 0, index)
+        squares_leaving = sends.shared((squares_in.at[: 2 * count - 1], first))
         for z_other, y_other in sources:
             for x_other in range(2):
                 away = jnp.logical_or(
                     jnp.logical_or(z != z_other, y != y_other), x != x_other
                 )
                 sends.start(
-                    squares_done.at[index],
-                    squares_in.at[squares_index, index],
-                    squares_sem.at[squares_index, index],
+                    squares_done.at[index, x_other],
+                    squares_in.at[index * count + source_index],
+                    squares_sem.at[index],
                     (z_other * 2 + x_other, y_other * 2 + core),
                     first,
                     away,
+                    leaving=squares_leaving,
                 )
 
     order = line_order(z, layers)
-
-    kinds = [(conv_in, conv_sem, 1, index) for index in range(2)]
-    kinds += [(memory_in, memory_sem, 0, index) for index in range(2)]
-    for inside, semaphores, home, index in kinds:
+    across = (1 - x) * 2 + core
+    across_leaving = sends.shared((three_pieces,))
+
+    def pass_on(distance, kind, index, *conditions):
+        inside, semaphores, home = kind
         part = slice(index * length, (index + 1) * length)
-        away = x != home
-        spot, sem = inside.at[z, part, :], semaphores.at[z, index]
-        arrived(spot, sem, away)
-        sends.start(spot, spot, sem, below, away, has_below)
-        sends.start(spot, spot, sem, above, away, has_above)
-    across = (1 - x) * 2 + core
+        if distance == 0:
+            away = x != home
+            spot, sem = inside.at[z, part, :], semaphores.at[z, index]
+            arrived(spot, sem, away, *conditions)
+            for device, further, leaving in (
+                (below, has_below, down_leaving),
+                (above, has_above, up_leaving),
+            ):
+                sends.start(spot, spot, sem, device, away, further, *conditions, leaving=leaving)
+            return
+        down, up = order[2 * distance - 2 : 2 * distance]
+        for (source, there, onward, further), leaving in ((down, up_leaving), (up, down_leaving)):
+            spot, sem = inside.at[source, part, :], semaphores.at[source, index]
+            arrived(spot, sem, there, *conditions)
+            device = (onward * 2 + x, tp)
+            sends.start(spot, spot, sem, device, there, further, *conditions, leaving=leaving)
+
+    def share_out(*conditions):
+        arrived(three_pieces, out_sem.at[across], *conditions)
+        for spot in (memory_out.at[across], conv_out.at[across]):
+            sends.start(spot, spot, out_sem.at[across], peer, *conditions, leaving=across_leaving)
+
+    convs, memories = (conv_in, conv_sem, 1), (memory_in, memory_sem, 0)
+    pass_on(0, convs, 0, first)
+    pass_on(0, convs, 1, first)
     for distance in range(1, layers):
-        for inside, semaphores, _, index in kinds:
-            part = slice(index * length, (index + 1) * length)
-            for source, there, onward, further in order[2 * distance - 2 : 2 * distance]:
-                spot, sem = inside.at[source, part, :], semaphores.at[source, index]
-                arrived(spot, sem, there)
-                sends.start(spot, spot, sem, (onward * 2 + x, tp), there, further)
-        if distance == 1:
-            for number in range(3):
-                spot, sem = out_piece(across, number)
-                arrived(spot, sem)
-                sends.start(spot, spot, sem, peer)
+        for kind in (memories, convs):
+            for index in range(2):
+                if distance + 1 < layers or index == 0:
+                    pass_on(distance, kind, index, first)
+        if distance == layers - 2:
+            share_out(first)
+    share_out(second)
+    for distance in range(1, layers + 2):
+        if distance < layers:
+            pass_on(distance, convs, 0, second)
+            pass_on(distance, convs, 1, second)
+        if 0 <= distance - 1 < layers:
+            pass_on(distance - 1, memories, 0, second)
+        if 0 <= distance - 2 < layers - 1:
+            pass_on(distance - 2, memories, 1, second)
     entries = layers * 2 * head_dim
     for index in range(2):
         part = slice(index * length, (index + 1) * length)
-        for z_other, y_other in sources:
-            own = jnp.logical_and(first, jnp.logical_and(z == z_other, y == y_other))
-            slot = y_other * layers + z_other
-            arrived(
-                squares_in.at[slot, index], squares_sem.at[slot, index], jnp.logical_not(own)
-            )
+        if index == 1:
+            pass_on(layers - 1, memories, 1)
+            pass_on(layers - 1, convs, 1, first)
+        at = index * count
+        arrived(squares_in.at[at : at + count - 1], squares_sem.at[index], first)
+        arrived(squares_in.at[at : at + count], squares_sem.at[index], second)
         if index == 0:
             for group in range(2):
-                part_out = group * 2 + 1 - core
-                for number in range(3):
-                    arrived(*out_piece(part_out, number))
-        total = squares_in[0, index]
+                arrived(three_pieces, out_sem.at[group * 2 + 1 - core])
+        total = squares_in[at]
         for slot in range(1, 2 * layers):
-            total = total + squares_in[slot, index]
-        total = pick(x, total[:, :length], total[:, length:])
-        row_scale = as_columns(lax.rsqrt(total * (1.0 / entries) + EPS))[:, 0:1]
+            total = total + squares_in[at + slot]
+        row_scale = stacked((lax.rsqrt(total * (1.0 / entries) + EPS),), length)
+        row_scale = as_columns(row_scale)[:, 0:1]
         for group in range(2):
             from_memory, from_conv = None, None
             for head in range(layers):
@@ -875,9 +951,9 @@
             partial[index, :, group * width : (group + 1) * width] = (
                 from_conv + row_scale * from_memory
             ).astype(bf16)
-        goal = ((core * 2 + index) * 2 + x, z)
+        device = ((core * 2 + index) * 2 + x, z)
         away = jnp.logical_or(core * 2 + index != z, tp != z)
-        sends.start(partial.at[index], slots.at[y], slot_sem.at[y], goal, away)
+        sends.start(partial.at[index], slots.at[y], slot_sem.at[y], device, away)
 
         @pl.when(jnp.logical_not(away))
         def _():
@@ -913,9 +989,9 @@
     channels = conv_value_weight.shape[1] // 2
     wide = features * columns
     rows = length * count // 2
+    span = rows // 2
     layers = count // 2
-    taps = conv_kernel.shape[0]
-    halo = -(-(taps - 1) // ROW_TILE) * ROW_TILE
+    halo = -(-(conv_kernel.shape[0] - 1) // ROW_TILE) * ROW_TILE
     width = memory_out_weight.shape[1]
     f32, bf16 = jnp.float32, jnp.bfloat16
     DMA = pltpu.SemaphoreType.DMA
@@ -923,17 +999,23 @@
     return pl.pallas_call(
         lambda *refs: layer_kernel(count, columns, *refs),
         out_shape=jax.ShapeDtypeStruct((2, length, features), bf16),
-        in_specs=[IN_VMEM] * 15,
+        in_specs=[pl.BlockSpec(memory_space=pltpu.HBM)] * 15,
         out_specs=IN_VMEM,
         scratch_shapes=[
+            V(tokens.shape, bf16),
+            V(query_weight.shape, bf16),
+            V(key_weight.shape, bf16),
+            V(value_weight.shape, bf16),
+            V(conv_value_weight.shape, bf16),
+            V(conv_gate_weight.shape, bf16),
+            V((2, 2, length), f32),
             V((rows, wide), bf16),
             V((wide, 2 * head_dim), bf16),
             V((rows, 2 * head_dim), f32),
             V(conv_kernel.shape, bf16),
             V((1, 2 * channels), f32),
             V((1, 2 * head_dim), f32),
-            V((2, wide), bf16),
-            V((2, wide), bf16),
+            V((2, 2, wide), bf16),
             V((4, 2, 2, length), f32),
             V((LANES, wide), f32),
             V((ROW_TILE, rows), f32),
@@ -941,38 +1023,42 @@
             V((2 * rows, head_dim), bf16),
             V((2 * rows, head_dim), bf16),
             V((rows, head_dim), bf16),
-            V((rows // 2, rows + rows // 2), f32),
-            V((rows // 2, 2 * rows), f32),
+            V((span, rows + span), f32),
+            V((span, 2 * rows), f32),
             V((rows, head_dim), bf16),
-            V((2, ROW_TILE, rows // 2), f32),
-            V((count, 2, ROW_TILE, rows // 2), f32),
+            V((2, 2, 1, length), f32),
+            V((2 * count, 1, length), f32),
             V((halo + rows, channels), f32),
             V((rows, channels), f32),
-            V((ROW_TILE, rows), f32),
-            V((count, ROW_TILE, rows), f32),
+            V((ROW_TILE, LANES), f32),
+            V((count, ROW_TILE, LANES), f32),
             V((rows, channels), bf16),
-            V((layers, rows // 2, head_dim), bf16),
-            V((layers, rows // 2, channels), bf16),
+            V((layers, span, head_dim), bf16),
+            V((layers, span, channels), bf16),
             V((4, 2 * head_dim, width), bf16),
             V((4, 2 * channels, width), bf16),
             V((2, length, features), bf16),
+            DMA((16,)),
             DMA((SENDS,)),
-            DMA((4, columns)),
+            DMA((4, 2)),
+            DMA((1,)),
             DMA((2, count)),
-            DMA((5,)),
             DMA((4,)),
             DMA((1,)),
-            DMA((2,)),
+            DMA((1,)),
+            DMA((1,)),
             DMA((2,)),
             DMA((1,)),
-            DMA((count,)),
-            DMA((count, 2)),
+            DMA((1,)),
+            DMA((2,)),
             DMA((layers, 2)),
             DMA((layers, 2)),
-            DMA((4, 3)),
+            DMA((4,)),
             DMA((2,)),
         ],
-        compiler_params=pltpu.CompilerParams(collective_id=0, has_side_effects=True),
+        compiler_params=pltpu.CompilerParams(
+            collective_id=0, has_side_effects=True
+        ),
     )(
         tokens,
         query_weight,
@@ -1006,7 +1092,7 @@
         count == 8
         and columns == 4
         and heads == count
-        and length % LANES == 0
+        and length == LANES
         and tokens.size * 2 <= 4 * 2**20
         and conv_value_weight.shape[1] * 2 == head_dim * heads
         and head_dim == 256

time: 80.3 us -> 72.9 us (0.908)
  the two profiles are of different devices: /device:TPU:13 before, /device:TPU:10 now
where the time goes in v3:
time: 72.9 us; the launch traced here: 72.7 us
  Pallas kernels  71.1 us (98%)
  other arithmetic  1.68 us (2%)
    pallas_call x1, Pallas kernels, layer(): pl.pallas_call(lambda *refs: layer_kernel(count, columns, *refs), out_sha...  71.1 us
    reduce_sum x1, other arithmetic, on_device_by_column(): return jnp.sum(slots.astype(jnp.float32), axis=0).astype(jnp.bfloat16)  1.68 us

profile of v3, /device:TPU:10, one launch (start us, length us, event | category | flops | bytes accessed | tf_op | source)
XLA Modules:
  0.0 72.7 jit_solution(17085688171304058681)
XLA Ops:
  0.0 71.1 %shard_map.145 = bf16[2,128,512]{2,1,0:T(8,128)(2,1)} custom-call(bf16[128,512]{1,0:T(8,128)(2,1)} %refs_0_.1, bf16[256,512]{1,0:T(8,128)(2,1)} %refs_1_.1, bf16[256,512]{1,0:T(8,128)(2,1)} %refs_2_.1, bf16[256,512]{1,0:T(8,128)(2,1)} %refs_3_.1, bf16[256,256]{1,0:T(8,128)(2,1)} %refs_4_.1, bf16[256,256]{1,0:T(8,128)(2,1)} %refs_5_.1, ...), custom_call_target="tpu_custom_call" | custom-call | tf_op jit(solution)/shard_map/pallas_call | solution.py:999
  71.1 1.7 %reduce_sum.12 = bf16[128,512]{1,0:T(8,128)(2,1)} reduce(bf16[2,128,512]{2,1,0:T(8,128)(2,1)} %shard_map.145, bf16[]{:T(256)} %constant.2.clone.1), dimensions={0}, to_apply=%region_0.0 | reduce | flops 65536 | bytes 393218 | tf_op jit(solution)/shard_map/reduce_sum | solution.py:1083

commit v4 on v3

--- a/solution.py
+++ b/solution.py
@@ -573,7 +573,10 @@
             sends.start(spot, spot, sem, onward, away, middle, leaving=z_leaving)
             sends.start(spot, spot, sem, x_side, away, leaving=x_leaving)
             sends.start(spot, spot, y_sem.at[0], y_side, away, leaving=y_leaving)
+    cross_leaving = [sends.shared((share,)) for _ in range(2)]
     send_weights(side, False, mate_leaving, near, middle)
+    send_weights(odd, True, cross_leaving[1], far)
+    send_weights(1 - odd, True, cross_leaving[0], far, ends)
     for _, _, i in groups:
         for j in range(2):
             spot, sem = block(i, y * 2 + j), token_sem.at[i, j]
@@ -581,13 +584,14 @@
             sends.start(spot, spot, y_sem.at[0], y_side, leaving=y_leaving)
 
     send_weights(side, False, mate_leaving, near, ends)
-    send_weights(1 - side, False, other_leaving, near)
-    for k in (jnp.where(near, 1 - side, 1 - odd), jnp.where(near, side, odd)):
-        send_weights(k, True, sends.shared((share,)))
-    for number in range(3):
-        send_out(number, first)
+    last = jnp.logical_and(middle, first)
+    send_weights(1 - side, False, other_leaving, near, jnp.logical_not(last))
+    k_cross = jnp.where(near, 1 - side, 1 - odd)
+    send_weights(k_cross, True, cross_leaving[0], jnp.logical_or(near, middle))
+    send_weights(side, True, cross_leaving[1], near)
+    send_weights(1 - side, False, other_leaving, near, last)
     for number in range(2):
-        send_out(number, second, near)
+        send_out(number, near)
 
     arrived(blocks(8), y_sem.at[0])
     for index, array in enumerate(own_arrays):
@@ -685,14 +689,18 @@
         other_unit(pair * 2 + 1)
         product[...] += multiply(pair * 2 * depth, 2 * depth)
 
+    for number in range(2):
+        send_out(number, first, far)
+    send_out(2, first)
+
     @pl.when(second)
     def _():
         queries[...] = product[:, :head_dim].astype(bf16)
 
     leaving = sends.shared((queries, second))
-    for index in range(2):
-        part = queries.at[index * span : (index + 1) * span, :]
-        sends.start(part, part, query_sem.at[index], x_side, second, leaving=leaving)
+    for number in range(4):
+        part = queries.at[number * length : (number + 1) * length, :]
+        sends.start(part, part, query_sem.at[number], x_side, second, leaving=leaving)
 
     @pl.when(first)
     def _():
@@ -797,58 +805,60 @@
     down_leaving = sends.shared(*((so_many(layers - at), z == at) for at in range(1, layers)))
     given_leaving = sends.shared((memory_in.at[0], first), (conv_in.at[0], second))
 
-    def spread(done, inside, semaphores, home, index):
-        here = x == home
-        kept = done.at[(2 * index + home) * length : (2 * index + home + 1) * length, :]
-        given = done.at[(2 * index + 1 - home) * length : (2 * index + 2 - home) * length, :]
+    def spread(done, inside, semaphores, home, number):
+        here, index = x == home, number // 2
+        source = done.at[number * length : (number + 1) * length, :]
         part = slice(index * length, (index + 1) * length)
         target, sem = inside.at[z, part, :], semaphores.at[z, index]
-        sends.start(given, target, sem, x_side, here, leaving=given_leaving)
-        sends.start(kept, target, sem, below, here, has_below, leaving=down_leaving)
-        sends.start(kept, target, sem, above, here, has_above, leaving=up_leaving)
+        if number % 2 != home:
+            sends.start(source, target, sem, x_side, here, leaving=given_leaving)
+            return
+        sends.start(source, target, sem, below, here, has_below, leaving=down_leaving)
+        sends.start(source, target, sem, above, here, has_above, leaving=up_leaving)
 
         @pl.when(here)
         def _():
-            inside[z, part, :] = kept[...]
-
-    for index in range(2):
-        spread(conv_done, conv_in, conv_sem, 1, index)
+            inside[z, part, :] = source[...]
+
+    for number in range(4):
+        spread(conv_done, conv_in, conv_sem, 1, number)
     for number in range(2):
         send_out(number, second, far)
     send_out(2, second)
 
     for array in (keys,):
         arrived(array, pair_sem.at[0], first, second_core)
-    for index in range(2):
-        arrived(
-            queries.at[index * span : (index + 1) * span, :], query_sem.at[index], first
-        )
+    for number in range(4):
+        start, index, inner = number * length, number // 2, number % 2
+        arrived(queries.at[start : start + length, :], query_sem.at[number], first)
 
         @pl.when(first)
         def _():
             width = reach[index]
             gain = memory_gain[...]
             gain = pick(odd, gain[:, :head_dim], gain[:, head_dim:])
-            for inner in range(2):
-                start = index * span + inner * length
-                scores = lax.dot_general(
-                    queries[start : start + length, :],
-                    keys[:width, :],
-                    NT,
-                    preferred_element_type=f32,
-                )
-                scores = scores * stores[index][inner * length : (inner + 1) * length, :]
-                numer = jnp.dot(
-                    scores.astype(bf16), values[:width, :], preferred_element_type=f32
-                )
-                denom = jnp.sum(scores, axis=1, keepdims=True)
-                cell = numer / jnp.maximum(jnp.abs(denom), 1.0)
-                memory_done[start : start + length, :] = (cell * gain).astype(bf16)
-                square = as_rows((jnp.sum(cell * cell, axis=1, keepdims=True),))
-                squares_done[index, inner] = square[0:1]
+            scores = lax.dot_general(
+                queries[start : start + length, :],
+                keys[:width, :],
+                NT,
+                preferred_element_type=f32,
+            )
+            scores = scores * stores[index][inner * length : (inner + 1) * length, :]
+            numer = jnp.dot(scores.astype(bf16), values[:width, :], preferred_element_type=f32)
+            denom = jnp.sum(scores, axis=1, keepdims=True)
+            cell = numer / jnp.maximum(jnp.abs(denom), 1.0)
+            memory_done[start : start + length, :] = (cell * gain).astype(bf16)
+            square = as_rows((jnp.sum(cell * cell, axis=1, keepdims=True),))
+            squares_done[index, inner] = square[0:1]
+
+        spread(memory_done, memory_in, memory_sem, 0, number)
+
+    @pl.when(first)
+    def _():
+        for index in range(2):
             squares_in[index * count + source_index] = squares_done[index, 0]
 
-        spread(memory_done, memory_in, memory_sem, 0, index)
+    for index in range(2):
         squares_leaving = sends.shared((squares_in.at[: 2 * count - 1], first))
         for z_other, y_other in sources:
             for x_other in range(2):
@@ -904,15 +914,16 @@
                     pass_on(distance, kind, index, first)
         if distance == layers - 2:
             share_out(first)
-    share_out(second)
     for distance in range(1, layers + 2):
         if distance < layers:
             pass_on(distance, convs, 0, second)
             pass_on(distance, convs, 1, second)
+        if 0 <= distance - 2 < layers - 1:
+            pass_on(distance - 2, memories, 1, second)
         if 0 <= distance - 1 < layers:
             pass_on(distance - 1, memories, 0, second)
-        if 0 <= distance - 2 < layers - 1:
-            pass_on(distance - 2, memories, 1, second)
+        if distance == layers - 1:
+            share_out(second)
     entries = layers * 2 * head_dim
     for index in range(2):
         part = slice(index * length, (index + 1) * length)
@@ -1047,7 +1058,7 @@
             DMA((1,)),
             DMA((1,)),
             DMA((1,)),
-            DMA((2,)),
+            DMA((4,)),
             DMA((1,)),
             DMA((1,)),
             DMA((2,)),
@@ -1057,24 +1068,29 @@
             DMA((2,)),
         ],
         compiler_params=pltpu.CompilerParams(
-            collective_id=0, has_side_effects=True
+            collective_id=0, has_side_effects=True, vmem_limit_bytes=40 * 2**20
         ),
     )(
-        tokens,
-        query_weight,
-        key_weight,
-        value_weight,
-        conv_value_weight,
-        conv_gate_weight,
-        conv_kernel,
-        conv_norm_gain.reshape(1, -1),
-        memory_norm_gain.reshape(1, -1),
-        input_gate_weight.T,
-        forget_gate_weight.T,
-        input_offset.T,
-        forget_offset.T,
-        memory_out_weight,
-        conv_out_weight,
+        *(
+            pltpu.with_memory_space_constraint(array, pltpu.HBM)
+            for array in (
+                tokens,
+                query_weight,
+                key_weight,
+                value_weight,
+                conv_value_weight,
+                conv_gate_weight,
+                conv_kernel,
+                conv_norm_gain.reshape(1, -1),
+                memory_norm_gain.reshape(1, -1),
+                input_gate_weight.T,
+                forget_gate_weight.T,
+                input_offset.T,
+                forget_offset.T,
+                memory_out_weight,
+                conv_out_weight,
+            )
+        )
     )
 
 

time: 72.9 us -> 67.7 us (0.929)
  Pallas kernels: 71.1 us -> 66.9 us
  other arithmetic: 1.68 us -> 0.71 us
    pallas_call x1, Pallas kernels: 71.1 us -> 66.9 us  [layer(): pl.pallas_call(lambda *refs: layer_kernel(count, columns, *refs), out_sha...]
    reduce_sum x1, other arithmetic: 1.68 us -> 0.71 us  [on_device_by_column(): return jnp.sum(slots.astype(jnp.float32), axis=0).astype(jnp.bfloat16)]
where the time goes in v4:
time: 67.7 us; the launch traced here: 67.6 us
  Pallas kernels  66.9 us (99%)
  other arithmetic  0.71 us (1%)
    pallas_call x1, Pallas kernels, layer(): pl.pallas_call(lambda *refs: layer_kernel(count, columns, *refs), out_sha...  66.9 us

profile of v4, /device:TPU:10, one launch (start us, length us, event | category | flops | bytes accessed | tf_op | source)
XLA Modules:
  0.0 67.6 jit_solution(17613918999848581830)
XLA Ops:
  0.0 66.9 %shard_map.145 = bf16[2,128,512]{2,1,0:T(8,128)(2,1)S(1)} custom-call(bf16[128,512]{1,0:T(8,128)(2,1)} %refs_0_.1, bf16[256,512]{1,0:T(8,128)(2,1)} %refs_1_.1, bf16[256,512]{1,0:T(8,128)(2,1)} %refs_2_.1, bf16[256,512]{1,0:T(8,128)(2,1)} %refs_3_.1, bf16[256,256]{1,0:T(8,128)(2,1)} %refs_4_.1, bf16[256,256]{1,0:T(8,128)(2,1)} %refs_5_.1, ...), custom_call_target="tpu_custom_call" | custom-call | tf_op jit(solution)/shard_map/pallas_call | solution.py:1010
  66.9 0.7 %reduce_sum.12 = bf16[128,512]{1,0:T(8,128)(2,1)} reduce(bf16[2,128,512]{2,1,0:T(8,128)(2,1)S(1)} %shard_map.145, bf16[]{:T(256)} %constant.2.clone.1), dimensions={0}, to_apply=%region_0.0 | reduce | flops 65536 | bytes 393218 | tf_op jit(solution)/shard_map/reduce_sum | solution.py:1099

commit v5 on v4

--- a/solution.py
+++ b/solution.py
@@ -591,7 +591,7 @@
     send_weights(side, True, cross_leaving[1], near)
     send_weights(1 - side, False, other_leaving, near, last)
     for number in range(2):
-        send_out(number, near)
+        send_out(number, near, second)
 
     arrived(blocks(8), y_sem.at[0])
     for index, array in enumerate(own_arrays):
@@ -690,8 +690,7 @@
         product[...] += multiply(pair * 2 * depth, 2 * depth)
 
     for number in range(2):
-        send_out(number, first, far)
-    send_out(2, first)
+        send_out(number, first, near)
 
     @pl.when(second)
     def _():
@@ -852,6 +851,9 @@
             squares_done[index, inner] = square[0:1]
 
         spread(memory_done, memory_in, memory_sem, 0, number)
+    for number in range(2):
+        send_out(number, first, far)
+    send_out(2, first)
 
     @pl.when(first)
     def _():

time: 67.7 us -> 66.4 us (0.981); the launches traced: 67.6 us -> 65.5 us
  Pallas kernels: 66.9 us -> 64.8 us
    pallas_call x1, Pallas kernels: 66.9 us -> 64.8 us  [layer(): pl.pallas_call(lambda *refs: layer_kernel(count, columns, *refs), out_sha...]
where the time goes in v5:
time: 66.4 us; the launch traced here: 65.5 us
  Pallas kernels  64.8 us (98%)
  other arithmetic  0.71 us (1%)
    pallas_call x1, Pallas kernels, layer(): pl.pallas_call(lambda *refs: layer_kernel(count, columns, *refs), out_sha...  64.8 us

profile of v5, /device:TPU:10, one launch (start us, length us, event | category | flops | bytes accessed | tf_op | source)
XLA Modules:
  0.0 65.5 jit_solution(10017330734459195864)
XLA Ops:
  0.0 64.8 %shard_map.145 = bf16[2,128,512]{2,1,0:T(8,128)(2,1)S(1)} custom-call(bf16[128,512]{1,0:T(8,128)(2,1)} %refs_0_.1, bf16[256,512]{1,0:T(8,128)(2,1)} %refs_1_.1, bf16[256,512]{1,0:T(8,128)(2,1)} %refs_2_.1, bf16[256,512]{1,0:T(8,128)(2,1)} %refs_3_.1, bf16[256,256]{1,0:T(8,128)(2,1)} %refs_4_.1, bf16[256,256]{1,0:T(8,128)(2,1)} %refs_5_.1, ...), custom_call_target="tpu_custom_call" | custom-call | tf_op jit(solution)/shard_map/pallas_call | solution.py:1012
  64.8 0.7 %reduce_sum.12 = bf16[128,512]{1,0:T(8,128)(2,1)} reduce(bf16[2,128,512]{2,1,0:T(8,128)(2,1)S(1)} %shard_map.145, bf16[]{:T(256)} %constant.2.clone.1), dimensions={0}, to_apply=%region_0.0 | reduce | flops 65536 | bytes 393218 | tf_op jit(solution)/shard_map/reduce_sum | solution.py:1101

commit v6 on v5

--- a/solution.py
+++ b/solution.py
@@ -697,7 +697,7 @@
         queries[...] = product[:, :head_dim].astype(bf16)
 
     leaving = sends.shared((queries, second))
-    for number in range(4):
+    for number in (0, 1, 3, 2):
         part = queries.at[number * length : (number + 1) * length, :]
         sends.start(part, part, query_sem.at[number], x_side, second, leaving=leaving)
 
@@ -827,7 +827,7 @@
 
     for array in (keys,):
         arrived(array, pair_sem.at[0], first, second_core)
-    for number in range(4):
+    for number in (0, 1, 3, 2):
         start, index, inner = number * length, number // 2, number % 2
         arrived(queries.at[start : start + length, :], query_sem.at[number], first)
 

time: 66.4 us -> 65.9 us (level)
  no operation moved by 1% of the time
where the time goes in v6:
time: 65.9 us; the launch traced here: 65.4 us
  Pallas kernels  64.6 us (98%)
  other arithmetic  0.71 us (1%)
    pallas_call x1, Pallas kernels, layer(): pl.pallas_call(lambda *refs: layer_kernel(count, columns, *refs), out_sha...  64.6 us

profile of v6, /device:TPU:10, one launch (start us, length us, event | category | flops | bytes accessed | tf_op | source)
XLA Modules:
  0.0 65.4 jit_solution(11410126288994303881)
XLA Ops:
  0.0 64.6 %shard_map.145 = bf16[2,128,512]{2,1,0:T(8,128)(2,1)S(1)} custom-call(bf16[128,512]{1,0:T(8,128)(2,1)} %refs_0_.1, bf16[256,512]{1,0:T(8,128)(2,1)} %refs_1_.1, bf16[256,512]{1,0:T(8,128)(2,1)} %refs_2_.1, bf16[256,512]{1,0:T(8,128)(2,1)} %refs_3_.1, bf16[256,256]{1,0:T(8,128)(2,1)} %refs_4_.1, bf16[256,256]{1,0:T(8,128)(2,1)} %refs_5_.1, ...), custom_call_target="tpu_custom_call" | custom-call | tf_op jit(solution)/shard_map/pallas_call | solution.py:1012
  64.6 0.7 %reduce_sum.12 = bf16[128,512]{1,0:T(8,128)(2,1)} reduce(bf16[2,128,512]{2,1,0:T(8,128)(2,1)S(1)} %shard_map.145, bf16[]{:T(256)} %constant.2.clone.1), dimensions={0}, to_apply=%region_0.0 | reduce | flops 65536 | bytes 393218 | tf_op jit(solution)/shard_map/reduce_sum | solution.py:1101

commit v7 on v6

--- a/solution.py
+++ b/solution.py
@@ -860,23 +860,6 @@
         for index in range(2):
             squares_in[index * count + source_index] = squares_done[index, 0]
 
-    for index in range(2):
-        squares_leaving = sends.shared((squares_in.at[: 2 * count - 1], first))
-        for z_other, y_other in sources:
-            for x_other in range(2):
-                away = jnp.logical_or(
-                    jnp.logical_or(z != z_other, y != y_other), x != x_other
-                )
-                sends.start(
-                    squares_done.at[index, x_other],
-                    squares_in.at[index * count + source_index],
-                    squares_sem.at[index],
-                    (z_other * 2 + x_other, y_other * 2 + core),
-                    first,
-                    away,
-                    leaving=squares_leaving,
-                )
-
     order = line_order(z, layers)
     across = (1 - x) * 2 + core
     across_leaving = sends.shared((three_pieces,))
@@ -909,6 +892,23 @@
     convs, memories = (conv_in, conv_sem, 1), (memory_in, memory_sem, 0)
     pass_on(0, convs, 0, first)
     pass_on(0, convs, 1, first)
+    for index in range(2):
+        squares_leaving = sends.shared((squares_in.at[: 2 * count - 1], first))
+        for z_other, y_other in sources:
+            for x_other in range(2):
+                away = jnp.logical_or(
+                    jnp.logical_or(z != z_other, y != y_other), x != x_other
+                )
+                sends.start(
+                    squares_done.at[index, x_other],
+                    squares_in.at[index * count + source_index],
+                    squares_sem.at[index],
+                    (z_other * 2 + x_other, y_other * 2 + core),
+                    first,
+                    away,
+                    leaving=squares_leaving,
+                )
+
     for distance in range(1, layers):
         for kind in (memories, convs):
             for index in range(2):

time: 65.9 us -> 66.1 us (level)
  no operation moved by 1% of the time
where the time goes in v7:
time: 66.1 us; the launch traced here: 65.4 us
  Pallas kernels  64.6 us (98%)
  other arithmetic  0.71 us (1%)
    pallas_call x1, Pallas kernels, layer(): pl.pallas_call(lambda *refs: layer_kernel(count, columns, *refs), out_sha...  64.6 us

profile of v7, /device:TPU:10, one launch (start us, length us, event | category | flops | bytes accessed | tf_op | source)
XLA Modules:
  0.0 65.4 jit_solution(4550013259238822412)
XLA Ops:
  0.0 64.6 %shard_map.145 = bf16[2,128,512]{2,1,0:T(8,128)(2,1)S(1)} custom-call(bf16[128,512]{1,0:T(8,128)(2,1)} %refs_0_.1, bf16[256,512]{1,0:T(8,128)(2,1)} %refs_1_.1, bf16[256,512]{1,0:T(8,128)(2,1)} %refs_2_.1, bf16[256,512]{1,0:T(8,128)(2,1)} %refs_3_.1, bf16[256,256]{1,0:T(8,128)(2,1)} %refs_4_.1, bf16[256,256]{1,0:T(8,128)(2,1)} %refs_5_.1, ...), custom_call_target="tpu_custom_call" | custom-call | tf_op jit(solution)/shard_map/pallas_call | solution.py:1012
  64.6 0.7 %reduce_sum.12 = bf16[128,512]{1,0:T(8,128)(2,1)} reduce(bf16[2,128,512]{2,1,0:T(8,128)(2,1)S(1)} %shard_map.145, bf16[]{:T(256)} %constant.2.clone.1), dimensions={0}, to_apply=%region_0.0 | reduce | flops 65536 | bytes 393218 | tf_op jit(solution)/shard_map/reduce_sum | solution.py:1101
